TPU v7x, 256 devices: a whole 4x4x8 slice. The times are simulated.
256 devices in a mesh: sp: 64 (over z, x, core), tp: 4 (over y).
Axes of the slice: x: 4, y: 4, z: 8, core: 2. Of those that a mesh axis runs over, the one named last changes fastest.
Arguments:
- cot_out: bfloat16 [16384, 2048], P('sp', 'tp'), may hold values from -16 to 16
- route_ids: int32 [16384, 2], P('sp'), may hold values from 0 to 63, all different within a row; in each aligned block of 256 rows (0 to 255, 256 to 511, ...) at most 12 rows name the same one
- route_weight: float32 [16384, 2], P('sp'), may hold values from 0.1 to 1
- expert_inputs: bfloat16 [64, 768, 2048], P('sp'), may hold values from -48 to 48
- w_gate: bfloat16 [64, 2048, 1024], P('sp', None, 'tp'), may hold values from -0.125 to 0.125
- w_up: bfloat16 [64, 2048, 1024], P('sp', None, 'tp'), may hold values from -0.125 to 0.125
- w_down: bfloat16 [64, 1024, 2048], P('sp', 'tp'), may hold values from -0.1875 to 0.1875
- w_proj: bfloat16 [2048, 2048], P('tp'), may hold values from -0.125 to 0.125
- conv_out: bfloat16 [16384, 2048], P('sp', 'tp'), may hold values from -6 to 6
- channel_norm_gain: float32 [2048], P('tp'), may hold values from 0.1 to 1.9
- taps: float32 [31, 2048], P(None, 'tp'), may hold values from -1 to 1
- value_pre: bfloat16 [16384, 2048], P('sp', 'tp'), may hold values from -6 to 6
- gate_pre: bfloat16 [16384, 2048], P('sp', 'tp'), may hold values from -6 to 6
Outputs:
- grad_gate_w: bfloat16 [64, 2048, 1024], P('sp', None, 'tp')
- grad_up_w: bfloat16 [64, 2048, 1024], P('sp', None, 'tp')
- grad_down_w: bfloat16 [64, 1024, 2048], P('sp', 'tp')
- grad_proj: float32 [2048, 2048], P(('tp', 'sp'))
- grad_value: bfloat16 [16384, 2048], P('sp', 'tp')
- grad_gate: bfloat16 [16384, 2048], P('sp', 'tp')
Inputs may be any that keep to these rules, and one draw needn't show every extreme that they name: `route_ids`: among the tokens of one index of sp no expert is chosen more than 12 times, a bound that some block reaches; a token's experts differ.
All inputs are finite; a program needn't handle non-finite values.
Results may differ from a plain program's by a relative error of at most 0.012.
Values may be sent and summed in bfloat16 or wider, within the bound.
A program may use at most 128 MiB of HBM per device.

v0:
```python
import jax
import jax.numpy as jnp
from jax import lax
from jax.sharding import Mesh
from jax.sharding import PartitionSpec as P

SP = ("sp_0", "sp_1", "sp_2")
TP_SP = ("tp", "sp_0", "sp_1", "sp_2")


clamp_limit = 7.0
swish_alpha = 1.702
norm_epsilon = 1e-05


def in_blocks(value, dim, devices):
    dims = value.shape
    tiles = value.reshape(*dims[:dim], devices, dims[dim] // devices, *dims[dim + 1 :])
    return jnp.moveaxis(tiles, dim, 0)


def sum_at_owner(value, axis, dim):
    tiles = in_blocks(value, dim, lax.axis_size(axis))
    arrived = lax.all_to_all(tiles, axis, split_axis=0, concat_axis=0, tiled=True)
    return arrived.astype(jnp.float32).sum(axis=0)


def from_everyone(value, axis):
    devices = lax.axis_size(axis)
    return lax.all_to_all(
        jnp.broadcast_to(value[None], (devices, *value.shape)), axis, 0, 0, tiled=True
    )


def in_order(tiles, dim):
    dims = list(tiles.shape[1:])
    dims[dim] *= tiles.shape[0]
    return jnp.moveaxis(tiles, 0, dim).reshape(dims)


def collect(value, axis, dim):
    tiles = from_everyone(value, axis)
    return in_order(tiles, dim)


def sum_by_axis(subtotal, axes):
    for axis in axes:
        subtotal = lax.psum_scatter(subtotal, axis, scatter_dimension=0, tiled=True)
    return subtotal


def of_everyone(value, axis):
    return from_everyone(value, axis).sum(axis=0)


def in_one(arrays, axis):
    flat, at, done = (jnp.concatenate([a.reshape(-1) for a in arrays]), 0, [])
    subtotal = of_everyone(flat, axis)
    for a in arrays:
        done.append(subtotal[at : at + a.size].reshape(a.shape))
        at += a.size
    return tuple(done)


def passed_along(value, axis, steps):
    count = lax.axis_size(axis)
    leading, last = (max(0, -steps), min(count, count - steps))
    return lax.ppermute(value, axis, [(source, source + steps) for source in range(leading, last)])


def per_device(
    cot_out,
    route_ids,
    route_weight,
    expert_inputs,
    w_gate,
    w_up,
    w_down,
    w_proj,
    conv_out,
    channel_norm_gain,
    taps,
    value_pre,
    gate_pre,
):
    group_size = lax.axis_size(SP)
    narrow_size = lax.axis_size("tp")
    tok_rows = cot_out.shape[0]
    chosen = route_ids.shape[1]
    slot_rows = expert_inputs.shape[1]
    capacity = slot_rows // group_size
    model_width = expert_inputs.shape[2]
    local_cols = cot_out.shape[1]
    flat_ids = route_ids.reshape(-1)
    expert_hot = (flat_ids[:, None] == jnp.arange(group_size, dtype=jnp.int32)[None, :]).astype(
        jnp.int32
    )
    earlier = jnp.sum((jnp.cumsum(expert_hot, axis=0) - expert_hot) * expert_hot, axis=1)
    dest_rows = flat_ids * capacity + earlier
    flat_weight = route_weight.reshape(-1)[:, None]
    scaled = (flat_weight * jnp.repeat(cot_out, chosen, axis=0).astype(jnp.float32)).astype(
        jnp.bfloat16
    )
    outgoing = (
        jnp.zeros((group_size * capacity, local_cols), jnp.bfloat16).at[dest_rows].set(scaled)
    )
    moved = lax.all_to_all(
        outgoing.reshape(group_size, capacity, local_cols),
        SP,
        split_axis=0,
        concat_axis=0,
        tiled=True,
    )
    arrived = lax.all_gather(moved, "tp", axis=2, tiled=True)
    rows_cot = arrived.reshape(slot_rows, model_width)
    rows_in = expert_inputs[0]
    gate_weight = w_gate[0]
    up_weight = w_up[0]
    down_weight = w_down[0]
    gate_lin = jnp.dot(rows_in, gate_weight, preferred_element_type=jnp.float32)
    up_lin = jnp.dot(rows_in, up_weight, preferred_element_type=jnp.float32)
    gate_c = jnp.minimum(gate_lin, clamp_limit)
    up_c = jnp.clip(up_lin, -clamp_limit, clamp_limit)
    sigma = jax.nn.sigmoid(swish_alpha * gate_c)
    act = ((up_c + 1.0) * gate_c * sigma).astype(jnp.bfloat16)
    grad_down = jnp.dot(act.T, rows_cot, preferred_element_type=jnp.float32).astype(jnp.bfloat16)
    d_act = jnp.dot(rows_cot, down_weight.T, preferred_element_type=jnp.float32)
    up_open = ((up_lin > -clamp_limit) & (up_lin < clamp_limit)).astype(jnp.float32)
    gate_open = (gate_lin < clamp_limit).astype(jnp.float32)
    d_up = (d_act * gate_c * sigma * up_open).astype(jnp.bfloat16)
    d_gate = (
        d_act * (up_c + 1.0) * (sigma + swish_alpha * gate_c * sigma * (1.0 - sigma)) * gate_open
    ).astype(jnp.bfloat16)
    grad_gate_part = jnp.dot(rows_in.T, d_gate, preferred_element_type=jnp.float32).astype(
        jnp.bfloat16
    )
    grad_up_part = jnp.dot(rows_in.T, d_up, preferred_element_type=jnp.float32).astype(jnp.bfloat16)
    partial_value = jnp.dot(d_gate, gate_weight.T, preferred_element_type=jnp.float32)
    partial_value = partial_value + jnp.dot(d_up, up_weight.T, preferred_element_type=jnp.float32)
    input_grad = sum_at_owner(partial_value.astype(jnp.bfloat16), "tp", 1).astype(jnp.bfloat16)
    coming = lax.all_to_all(
        input_grad.reshape(group_size, capacity, local_cols),
        SP,
        split_axis=0,
        concat_axis=0,
        tiled=True,
    )
    picked = coming.reshape(group_size * capacity, local_cols)[dest_rows].astype(jnp.float32)
    summed = jnp.sum(picked.reshape(tok_rows, chosen, local_cols), axis=1)
    mix_grad = (cot_out.astype(jnp.float32) + summed).astype(jnp.bfloat16)
    mix_full = collect(mix_grad, "tp", 1)
    convolution_filter = conv_out.astype(jnp.float32)
    channel_total = local_cols * narrow_size
    first_sum, square_sum = lax.psum(
        (
            jnp.sum(convolution_filter, axis=1),
            jnp.sum(convolution_filter * convolution_filter, axis=1),
        ),
        "tp",
    )
    channel_mean = (first_sum / channel_total)[:, None]
    var = (square_sum / channel_total)[:, None] - channel_mean * channel_mean
    inverse_deviation = lax.rsqrt(var + norm_epsilon)
    normalized_input = (convolution_filter - channel_mean) * inverse_deviation
    normalized_output = normalized_input * channel_norm_gain[None, :]
    sigma_conv = jax.nn.sigmoid(normalized_output)
    act_conv = (normalized_output * sigma_conv).astype(jnp.bfloat16)
    grad_proj = sum_by_axis(
        lax.dot_general(
            act_conv, mix_full, (((0,), (0,)), ((), ())), preferred_element_type=jnp.float32
        ),
        SP,
    )
    d_act_conv = jnp.dot(mix_full, w_proj.T, preferred_element_type=jnp.float32)
    normalized_gradient = (
        d_act_conv
        * sigma_conv
        * (1.0 + normalized_output * (1.0 - sigma_conv))
        * channel_norm_gain[None, :]
    )
    first_term_gradient, second_term_gradient = in_one(
        (
            jnp.sum(normalized_gradient, axis=1),
            jnp.sum(normalized_gradient * normalized_input, axis=1),
        ),
        "tp",
    )
    convolution_gradient = inverse_deviation * (
        normalized_gradient
        - (first_term_gradient / channel_total)[:, None]
        - normalized_input * (second_term_gradient / channel_total)[:, None]
    )
    reach = taps.shape[0]
    following = passed_along(convolution_gradient[: reach - 1], SP, -1)
    extended = jnp.concatenate([convolution_gradient, following], axis=0)
    d_glu = jnp.zeros_like(convolution_gradient)
    for offset in range(reach):
        begin = reach - 1 - offset
        d_glu = d_glu + taps[offset][None, :] * extended[begin : begin + tok_rows]
    gate_sig = jax.nn.sigmoid(gate_pre.astype(jnp.float32))
    grad_value = (d_glu * gate_sig).astype(jnp.bfloat16)
    grad_gate = (d_glu * value_pre.astype(jnp.float32) * gate_sig * (1.0 - gate_sig)).astype(
        jnp.bfloat16
    )
    return (
        grad_gate_part[None],
        grad_up_part[None],
        grad_down[None],
        grad_proj,
        grad_value,
        grad_gate,
    )


def solution(mesh):
    finer = Mesh(mesh.devices.reshape(8, 4, 2, mesh.shape["tp"]), ("sp_0", "sp_1", "sp_2", "tp"))
    placed = (
        P(SP, "tp"),
        P(SP, None),
        P(SP, None),
        P(SP, None, None),
        P(SP, None, "tp"),
        P(SP, None, "tp"),
        P(SP, "tp", None),
        P("tp", None),
        P(SP, "tp"),
        P("tp"),
        P(None, "tp"),
        P(SP, "tp"),
        P(SP, "tp"),
    )
    return jax.shard_map(
        per_device,
        mesh=finer,
        in_specs=placed,
        out_specs=(
            P(SP, None, "tp"),
            P(SP, None, "tp"),
            P(SP, "tp", None),
            P(TP_SP, None),
            P(SP, "tp"),
            P(SP, "tp"),
        ),
        check_vma=False,
    )
```

profile of v0, /device:TPU:2, one launch (start us, length us, event | category | flops | bytes accessed | tf_op | source)
XLA Modules:
  0.0 351.1 jit_solution(16087362731274032509)
XLA Ops:
  7.2 0.8 broadcast_multiply_fusion
  8.1 0.9 copy.48
  9.6 1.2 reduce-window.6
  11.0 2.2 broadcast_in_dim.15
  13.2 2.9 convert_element_type.80
  16.6 4.1 %scatter_custom_fusion = bf16[768,512]{1,0:T(8,128)(2,1)} fusion(s32[512]{0:T(512)S(1)} %bitcast.147, f32[512,512]{1,0:T(8,128)} %convert_element_type.80, f32[512]{0:T(512)S(1)} %mul.447, bf16[]{:T(256)} %constant.12.clone.1), kind=kCustom, calls=%fused_computation.199 | custom fusion | flops 524288 | bytes 1837058 | tf_op jit(solution)/shard_map/scatter | solution.py:105
  20.6 2.1 reshape.100
  22.7 40.9 %all_to_all.26 = bf16[64,12,512]{2,1,0:T(8,128)(2,1)} all-to-all(bf16[64,12,512]{2,1,0:T(8,128)(2,1)} %reshape.100), channel_id=1, replica_groups=mesh['sp_0'=8,'sp_1'=4,'sp_2'=2,'tp'=4] {'sp_0','sp_1','sp_2'}, dimensions={0} | all-to-all | bytes 1572864 | tf_op jit(solution)/shard_map/all_to_all | solution.py:107
  63.7 3.2 fusion.4
  66.8 1.9 fusion.6
  68.7 42.5 %all-gather.2.cloned.1.call-done = bf16[64,12,2048]{2,1,0:T(8,128)(2,1)} async-done(((bf16[64,12,512]{2,1,0:T(8,128)(2,1)}), bf16[64,12,2048]{2,1,0:T(8,128)(2,1)}) %all-gather.2.cloned.1.call-update) | async-done | bytes 3145744 | tf_op jit(solution)/shard_map/all_gather | solution.py:114
  111.2 6.2 %reshape.101 = bf16[768,2048]{1,0:T(8,128)(2,1)} reshape(bf16[64,12,2048]{2,1,0:T(8,128)(2,1)} %all-gather.2.cloned.1.call-done) | data formatting | bytes 6291456 | tf_op jit(solution)/shard_map/reshape | solution.py:115
  117.3 4.1 %select_convert_fusion = (bf16[768,256]{1,0:T(8,128)(2,1)S(1)}, bf16[768,256]{1,0:T(8,128)(2,1)S(1)}) fusion(f32[768,256]{1,0:T(8,128)} %fusion.4, f32[768,256]{1,0:T(8,128)} %fusion.6, bf16[768,2048]{1,0:T(8,128)(2,1)} %reshape.101, bf16[1,256,2048]{2,1,0:T(8,128)(2,1)} %param.19), kind=kOutput, calls=%fused_computation.62 | convolution fusion | flops 809828352 | bytes 6553600 | tf_op jit(solution)/shard_map/dot_general | solution.py:127
  121.5 1.0 fusion.27
  123.0 1.0 add_convert_fusion
  124.3 41.0 %all_to_all.27 = bf16[4,768,512]{2,1,0:T(8,128)(2,1)} all-to-all(bf16[4,768,512]{2,1,0:T(8,128)(2,1)S(1)} %bitcast.113), channel_id=1, replica_groups=mesh['sp_0'=8,'sp_1'=4,'sp_2'=2,'tp'=4] {'tp'}, dimensions={0} | all-to-all | bytes 6291456 | tf_op jit(solution)/shard_map/all_to_all | solution.py:24
  165.3 3.5 reduce_sum.81
  168.8 2.1 reshape.103
  170.8 10.7 %all-to-all-start.2 = ((bf16[64,12,512]{2,1,0:T(8,128)(2,1)}), bf16[64,12,512]{2,1,0:T(8,128)(2,1)}, u32[]{:S(2)}, u32[]{:S(2)}) async-start(bf16[64,12,512]{2,1,0:T(8,128)(2,1)} %reshape.103), calls=%async_computation.2 | async-start | bytes 2097152 | tf_op jit(solution)/shard_map/all_to_all | solution.py:141
  181.6 28.7 %all-to-all-done.2 = bf16[64,12,512]{2,1,0:T(8,128)(2,1)} async-done(((bf16[64,12,512]{2,1,0:T(8,128)(2,1)}), bf16[64,12,512]{2,1,0:T(8,128)(2,1)}, u32[]{:S(2)}, u32[]{:S(2)}) %all-to-all-start.2) | async-done | bytes 786464 | tf_op jit(solution)/shard_map/all_to_all | solution.py:141
  210.3 2.1 reshape.104
  212.3 3.9 %gather_fusion = bf16[512,512]{1,0:T(8,128)(2,1)} fusion(bf16[768,512]{1,0:T(8,128)(2,1)} %reshape.104, s32[1024]{0:T(1024)S(1)} %pad_clamp_fusion), kind=kCustom, calls=%fused_computation | custom fusion | bytes 1050624 | tf_op jit(solution)/shard_map/gather | solution.py:148
  216.2 2.7 reshape.106
  218.9 3.3 reduce_sum.82
  222.2 1.9 add_convert_fusion.1
  224.1 1.8 copy.53
  225.8 2.0 broadcast_in_dim.19
  227.8 4.2 %all-to-all-start.3 = ((bf16[4,256,512]{1,2,0:T(8,128)(2,1)}), bf16[4,256,512]{1,2,0:T(8,128)(2,1)}, u32[]{:S(2)}, u32[]{:S(2)}) async-start(bf16[4,256,512]{1,2,0:T(8,128)(2,1)} %broadcast_in_dim.19), calls=%async_computation.3 | async-start | bytes 2097152 | tf_op jit(solution)/shard_map/all_to_all | solution.py:30
  232.3 16.4 %all-reduce = (f32[256]{0:T(256)S(1)}, f32[256]{0:T(256)S(1)}) all-reduce(f32[256]{0:T(256)S(1)} %get-tuple-element.39, f32[256]{0:T(256)S(1)} %get-tuple-element.38), channel_id=1, replica_groups=mesh['sp_0'=8,'sp_1'=4,'sp_2'=2,'tp'=4] {'tp'}, use_global_device_ids=true, to_apply=%region_7.8 | all-reduce | flops 512 | bytes 4096 | tf_op jit(solution)/shard_map/psum | solution.py:154
  248.7 4.1 %fusion.142 = f32[512,2048]{1,0:T(8,128)} fusion(bf16[256,2048]{0,1:T(8,128)(2,1)} %bitcast.14, bf16[256,512]{1,0:T(8,128)(2,1)S(1)} %copy-done.2, f32[512]{0:T(512)S(1)} %copy-done.11, f32[256]{0:T(256)S(1)} %get-tuple-element.80, f32[256]{0:T(256)S(1)} %get-tuple-element.79), kind=kOutput, calls=%fused_computation.212 | convolution fusion | flops 538050560 | bytes 5509120 | tf_op jit(solution)/shard_map/dot_general | solution.py:169
  252.9 0.8 copy-done.9
  253.7 0.6 fusion.160
  254.3 0.7 fusion.159
  255.0 4.6 %fusion.14 = bf16[1,256,2048]{2,1,0:T(8,128)(2,1)} fusion(bf16[768,2048]{1,0:T(8,128)(2,1)} %reshape.101, f32[768,256]{1,0:T(8,128)} %fusion.6, f32[768,256]{1,0:T(8,128)} %fusion.4), kind=kOutput, calls=%fused_computation.44 | convolution fusion | flops 807796736 | bytes 5767168 | tf_op jit(solution)/shard_map/dot_general | solution.py:126
  259.6 3.0 fusion.157
  263.2 3.2 all-to-all-start.4
  266.5 37.2 %reduce-scatter.4.cloned.1.call-done = f32[64,2048]{1,0:T(8,128)} async-done(((f32[512,2048]{1,0:T(8,128)}), f32[64,2048]{1,0:T(8,128)}) %reduce-scatter.4.cloned.1.call-update) | async-done | bytes 524304 | tf_op jit(solution)/shard_map/reduce_scatter | solution.py:48
  303.8 3.0 fusion.18
  306.8 1.2 fusion.132
  308.0 0.8 copy-done.1
  308.8 2.1 collective-permute-start
  311.0 3.0 fusion.15
  314.0 2.3 copy.55
  316.3 2.3 copy.56
  318.5 8.5 %reduce-scatter.6.cloned.1.call-done = f32[16,2048]{1,0:T(8,128)} async-done(((f32[64,2048]{1,0:T(8,128)}), f32[16,2048]{1,0:T(8,128)}) %reduce-scatter.6.cloned.1.call-update) | async-done | bytes 131088 | tf_op jit(solution)/shard_map/reduce_scatter | solution.py:48
  327.1 11.4 %multiply_convert_fusion.3 = (bf16[256,512]{1,0:T(8,128)(2,1)}, f32[256,512]{1,0:T(8,128)S(1)}) fusion(bf16[256,512]{1,0:T(8,128)(2,1)} %param.24, bf16[256,512]{1,0:T(8,128)(2,1)S(1)} %copy-done.6, f32[256,512]{1,0:T(8,128)} %copy-done.1, f32[512]{0:T(512)} %bitcast.125, f32[30,512]{1,0:T(8,128)S(1)} %collective-permute-done, f32[512]{0:T(512)} %bitcast.126, ...), kind=kLoop, calls=%fused_computation.202 | loop fusion | flops 13238272 | bytes 1959936 | tf_op jit(solution)/shard_map/convert_element_type | solution.py:202
  338.4 0.9 multiply_convert_fusion.4
  339.3 5.3 %reduce-scatter.8.cloned.1.call-done = f32[8,2048]{1,0:T(8,128)} async-done(((f32[16,2048]{1,0:T(8,128)}), f32[8,2048]{1,0:T(8,128)}) %reduce-scatter.8.cloned.1.call-update) | async-done | bytes 65552 | tf_op jit(solution)/shard_map/reduce_scatter | solution.py:48
  (56 shorter events, 3.1 us)
Async XLA Ops:
  7.2 56.5 %copy-start = (bf16[1,768,2048]{2,1,0:T(8,128)(2,1)S(1)}, bf16[1,768,2048]{2,1,0:T(8,128)(2,1)}, u32[]{:S(2)}) copy-start(bf16[1,768,2048]{2,1,0:T(8,128)(2,1)} %param.16) | copy-start | bytes 9437188
  7.2 9.0 %copy-start.10 = (f32[256,2]{0,1:T(2,128)S(1)}, f32[256,2]{0,1:T(2,128)}, u32[]{:S(2)}) copy-start(f32[256,2]{0,1:T(2,128)} %param.15) | copy-start | bytes 6148
  7.2 104.0 %all-gather.2.cloned.1.call-start = ((), (), s32[]{:S(2)}) async-start(), calls=%async_computation.8 | async-start | bytes 5242880 | tf_op jit(solution)/shard_map/all_gather | solution.py:114
  63.6 3.2 copy-start.4
  117.3 4.2 %copy-start.5 = (bf16[1,2048,256]{2,1,0:T(8,128)(2,1)S(1)}, bf16[1,2048,256]{2,1,0:T(8,128)(2,1)}, u32[]{:S(2)}) copy-start(bf16[1,2048,256]{2,1,0:T(8,128)(2,1)} %param.17) | copy-start | bytes 3145732
  121.5 1.1 copy-start.3
  121.5 1.1 copy-start.8
  121.5 1.5 copy-start.7
  170.8 39.4 %all-to-all-start.2 = ((bf16[64,12,512]{2,1,0:T(8,128)(2,1)}), bf16[64,12,512]{2,1,0:T(8,128)(2,1)}, u32[]{:S(2)}, u32[]{:S(2)}) async-start(bf16[64,12,512]{2,1,0:T(8,128)(2,1)} %reshape.103), calls=%async_computation.2 | async-start | bytes 2097152 | tf_op jit(solution)/shard_map/all_to_all | solution.py:141
  218.9 13.3 %copy-start.2 = (bf16[256,512]{1,0:T(8,128)(2,1)S(1)}, bf16[256,512]{1,0:T(8,128)(2,1)}, u32[]{:S(2)}) copy-start(bf16[256,512]{1,0:T(8,128)(2,1)} %param.21) | copy-start | bytes 786436
  218.9 29.8 %copy-start.11 = (f32[512]{0:T(512)S(1)}, f32[512]{0:T(512)}, u32[]{:S(2)}) copy-start(f32[512]{0:T(512)} %param.22) | copy-start | bytes 6148
  227.8 20.9 %all-to-all-start.3 = ((bf16[4,256,512]{1,2,0:T(8,128)(2,1)}), bf16[4,256,512]{1,2,0:T(8,128)(2,1)}, u32[]{:S(2)}, u32[]{:S(2)}) async-start(bf16[4,256,512]{1,2,0:T(8,128)(2,1)} %broadcast_in_dim.19), calls=%async_computation.3 | async-start | bytes 2097152 | tf_op jit(solution)/shard_map/all_to_all | solution.py:30
  232.1 71.6 %reduce-scatter.4.cloned.1.call-start = ((), (), s32[]{:S(2)}) async-start(), calls=%async_computation.9 | async-start | bytes 4718592 | tf_op jit(solution)/shard_map/reduce_scatter | solution.py:48
  252.8 0.8 copy-start.9
  255.0 4.6 %copy-start.12 = (bf16[512,2048]{1,0:T(8,128)(2,1)S(1)}, bf16[512,2048]{1,0:T(8,128)(2,1)}, u32[]{:S(2)}) copy-start(bf16[512,2048]{1,0:T(8,128)(2,1)} %param.20) | copy-start | bytes 6291460
  263.2 43.5 %all-to-all-start.4 = ((f32[4,1,512]{2,1,0:T(1,128)}), f32[4,1,512]{2,1,0:T(1,128)S(1)}, u32[]{:S(2)}, u32[]{:S(2)}) async-start(f32[4,1,512]{2,1,0:T(1,128)} %broadcast_in_dim.20), calls=%async_computation.7 | async-start | bytes 16384 | tf_op jit(solution)/shard_map/all_to_all | solution.py:30
  266.5 60.5 %reduce-scatter.6.cloned.1.call-start = ((), (), s32[]{:S(2)}) async-start(), calls=%async_computation.10 | async-start | bytes 655360 | tf_op jit(solution)/shard_map/reduce_scatter | solution.py:48
  303.7 40.9 %reduce-scatter.8.cloned.1.call-start = ((), (), s32[]{:S(2)}) async-start(), calls=%async_computation.11 | async-start | bytes 196608 | tf_op jit(solution)/shard_map/reduce_scatter | solution.py:48
  308.0 0.8 copy-start.1
  308.8 18.2 %collective-permute-start = (f32[30,512]{1,0:T(8,128)S(1)}, f32[30,512]{1,0:T(8,128)S(1)}, u32[]{:S(2)}, u32[]{:S(2)}) collective-permute-start(f32[30,512]{1,0:T(8,128)S(1)} %slice.267), channel_id=1, source_target_pairs={{4,0},{8,4},{12,8},{16,12},{20,16},{24,20},{28,24},{32,28},{36,32}... | collective-permute-start | bytes 184328 | tf_op jit(solution)/shard_map/ppermute | solution.py:68
  314.0 13.1 %copy-start.6 = (bf16[256,512]{1,0:T(8,128)(2,1)S(1)}, bf16[256,512]{1,0:T(8,128)(2,1)}, u32[]{:S(2)}) copy-start(bf16[256,512]{1,0:T(8,128)(2,1)} %param.25) | copy-start | bytes 786436
Sparse Core Ops, SparseCore 0:
  63.8 47.3 all-gather.1
  253.0 50.6 reduce-scatter.3
  306.2 20.7 reduce-scatter.5
  329.9 14.6 reduce-scatter.7
where the time goes:
time: 354 us; the launch traced here: 351 us
  waiting for transfers between devices  122 us (34%)
  blocking collectives  98.3 us (28%)
  local copies, waits for them, and re-layouts  38.6 us (11%)
  matrix products  28.9 us (8%)
  other arithmetic  28.6 us (8%)
  starting transfers between devices  20.5 us (6%)
  between operations  14.1 us (4%)
    reduce_scatter x3, waiting for transfers between devices, sum_by_axis(): subtotal = lax.psum_scatter(subtotal, axis, scatter_dimension=0, tiled=True)  51 us
    all_gather x1, waiting for transfers between devices, per_device(): arrived = lax.all_gather(moved, 'tp', axis=2, tiled=True)  42.5 us
    all_to_all x1, blocking collectives, sum_at_owner(): lax.all_to_all(tiles, axis, split_axis=0, concat_axis=0, tiled=True)  41 us
    all_to_all x1, blocking collectives, per_device(): lax.all_to_all(outgoing.reshape(group_size, capacity, local_cols), SP, sp...  40.9 us
    all_to_all x1, waiting for transfers between devices, per_device(): lax.all_to_all(input_grad.reshape(group_size, capacity, local_cols), SP,...  28.7 us
    psum x1, blocking collectives, per_device(): lax.psum((jnp.sum(convolution_filter, axis=1), jnp.sum(convolution_filter...  16.4 us
    convert_element_type x1, other arithmetic, per_device(): (d_glu * value_pre.astype(jnp.float32) * gate_sig * (1.0 - gate_sig)).ast...  11.4 us
    all_to_all x1, starting transfers between devices, per_device(): lax.all_to_all(input_grad.reshape(group_size, capacity, local_cols), SP,...  10.7 us
  transfers between devices with their start and end apart: 8, of which 5 were waited for; matrix products, arithmetic and copies ran while one was open for 11% of the time, Pallas kernels for 0%

commit v1 on v0

--- a/solution.py
+++ b/solution.py
@@ -1,16 +1,326 @@
 import jax
 import jax.numpy as jnp
 from jax import lax
+from jax.experimental import pallas as pl
+from jax.experimental.pallas import tpu as pltpu
 from jax.sharding import Mesh
 from jax.sharding import PartitionSpec as P
 
 SP = ("sp_0", "sp_1", "sp_2")
 TP_SP = ("tp", "sp_0", "sp_1", "sp_2")
-
+MESH = pl.DeviceIdType.MESH
 
 clamp_limit = 7.0
 swish_alpha = 1.702
 norm_epsilon = 1e-05
+
+CH = 4
+LANES = 128
+NZ = 8
+NG = 8
+NY = 4
+CAP = 12
+BLOCK = NZ * CAP
+ROWS = NZ * BLOCK
+HALF = ROWS // 2
+TOK = 256
+WIDE = CH * LANES
+HID = 256
+BF = jnp.bfloat16
+F32 = jnp.float32
+
+
+def nt(a, b):
+    return lax.dot_general(a, b, (((1,), (1,)), ((), ())), preferred_element_type=F32)
+
+
+def tn(a, b):
+    return lax.dot_general(a, b, (((0,), (0,)), ((), ())), preferred_element_type=F32)
+
+
+def nn(a, b):
+    return lax.dot_general(a, b, (((1,), (0,)), ((), ())), preferred_element_type=F32)
+
+
+def wait_all(ref, sem):
+    pltpu.make_async_copy(ref, ref, sem).wait()
+
+
+def send(src, dst, send_sem, recv_sem, device):
+    pltpu.make_async_remote_copy(
+        src_ref=src,
+        dst_ref=dst,
+        send_sem=send_sem,
+        recv_sem=recv_sem,
+        device_id=device,
+        device_id_type=MESH,
+    ).start()
+
+
+def lanes(c):
+    return pl.ds(c * LANES, LANES)
+
+
+def rows_of(block):
+    return pl.ds(pl.multiple_of(block * BLOCK, BLOCK), BLOCK)
+
+
+def moe_kernel(
+    cot, ids_c, ids_r, w_r, rows_in, wg, wu, wd, perm,
+    gg_out, gu_out, gd_out, mix,
+    out_a, recv_a, out_b, cotf, act_s, f_up, f_gate, dact, dgu, sel_t, rows_p,
+    partial, r1l, r1r, accl, accr, from_l, from_r, egrad, recv_b2, out_a2, coming,
+    s_a, r_a, s_b, r_b, s_y, r_yl, r_yr, r_fl, r_fr,
+    s_rs, r_1l, r_1r, r_sl, r_sr, s_b2, r_b2, s_a2, r_a2, s_m, r_ml, r_mr, r_nl, r_nr,
+):
+    z = lax.axis_index("sp_0")
+    g = lax.axis_index("sp_1") * 2 + lax.axis_index("sp_2")
+    y = lax.axis_index("tp")
+    right, left, across = lax.rem(y + 1, NY), lax.rem(y + 3, NY), lax.rem(y + 2, NY)
+    to_right, to_left = {"tp": right}, {"tp": left}
+
+    def z_peer(step):
+        peer = lax.rem(z + step, NZ)
+        return peer, {"sp_0": peer}
+
+    def g_peer(step):
+        peer = lax.rem(g + step, NG)
+        return peer, {"sp_1": peer // 2, "sp_2": lax.rem(peer, 2)}
+
+    barrier = pltpu.get_barrier_semaphore()
+    for step in range(1, NZ):
+        pl.semaphore_signal(barrier, inc=1, device_id=z_peer(step)[1], device_id_type=MESH)
+        pl.semaphore_signal(barrier, inc=1, device_id=g_peer(step)[1], device_id_type=MESH)
+    for device in (to_right, to_left):
+        pl.semaphore_signal(barrier, inc=1, device_id=device, device_id_type=MESH)
+
+    t_sub = lax.broadcasted_iota(jnp.int32, (TOK, TOK), 0)
+    t_lane = lax.broadcasted_iota(jnp.int32, (TOK, TOK), 1)
+    before, after = t_sub < t_lane, t_lane < t_sub
+    col = [ids_c[:, k : k + 1] for k in (0, 1)]
+    row = [ids_r[k : k + 1, :] for k in (0, 1)]
+    slot_r = lax.broadcasted_iota(jnp.int32, (ROWS, TOK), 0).astype(F32)
+    slot_c = lax.broadcasted_iota(jnp.int32, (TOK, ROWS), 1).astype(F32)
+    chosen, weight, back = None, None, None
+    for k in (0, 1):
+        same = ((col[0] == row[k]) | (col[1] == row[k])) & before
+        dest = jnp.sum(jnp.where(same, 1.0, 0.0), axis=0, keepdims=True) + CAP * row[k]
+        hot = slot_r == dest
+        one, scale = jnp.where(hot, 1.0, 0.0), jnp.where(hot, w_r[k : k + 1, :], 0.0)
+        chosen = one if chosen is None else chosen + one
+        weight = scale if weight is None else weight + scale
+        same = ((row[0] == col[k]) | (row[1] == col[k])) & after
+        dest = jnp.sum(jnp.where(same, 1.0, 0.0), axis=1, keepdims=True) + CAP * col[k]
+        one = jnp.where(slot_c == dest, 1.0, 0.0)
+        back = one if back is None else back + one
+    chosen = chosen.astype(BF)
+    weight = jnp.sum(weight, axis=1, keepdims=True)
+    sel_t[...] = back.astype(BF)
+
+    pl.semaphore_wait(barrier, NZ - 1 + NG - 1 + 2)
+
+    for c in range(CH):
+        picked = nn(chosen, cot[:, lanes(c)])
+        out_a[c] = (weight * picked).astype(BF)
+        for step in (4, 3, 5, 2, 6, 1, 7):
+            peer, device = z_peer(step)
+            send(out_a.at[c, rows_of(peer)], recv_a.at[c, rows_of(z)], s_a.at[c], r_a.at[c], device)
+        recv_a[c, rows_of(z), :] = out_a[c, rows_of(z), :]
+
+    for j in range(8):
+        cols = pl.ds(j * 256, 256)
+        rows_p[:, cols] = nn(perm[...], rows_in[:, cols]).astype(BF)
+    for j in range(3):
+        part = pl.ds(j * 256, 256)
+        gate_lin = nn(rows_p[part, :], wg[...])
+        up_lin = nn(rows_p[part, :], wu[...])
+        gate_c = jnp.minimum(gate_lin, clamp_limit)
+        up_c = jnp.clip(up_lin, -clamp_limit, clamp_limit)
+        sig = jax.nn.sigmoid(swish_alpha * gate_c)
+        act_s[part, :] = ((up_c + 1.0) * gate_c * sig).astype(BF)
+        up_open = (up_lin > -clamp_limit) & (up_lin < clamp_limit)
+        f_up[part, :] = jnp.where(up_open, gate_c * sig, 0.0)
+        slope = (up_c + 1.0) * (sig + swish_alpha * gate_c * sig * (1.0 - sig))
+        f_gate[part, :] = jnp.where(gate_lin < clamp_limit, slope, 0.0)
+
+    for s in range(CH + 3):
+        c = s
+        if 0 <= c < CH:
+            wait_all(recv_a.at[c, pl.ds(0, ROWS - BLOCK)], r_a.at[c])
+            out_b[c] = nn(perm[...], recv_a[c]).astype(BF)
+            for step in (4, 2, 6, 3, 5, 1, 7):
+                peer, device = g_peer(step)
+                send(
+                    out_b.at[c, rows_of(peer)], cotf.at[y, rows_of(g), lanes(c)],
+                    s_b.at[c], r_b.at[c], device,
+                )
+            cotf[y, rows_of(g), lanes(c)] = out_b[c, rows_of(g), :]
+        c = s - 1
+        if 0 <= c < CH:
+            wait_all(out_b.at[c, pl.ds(0, ROWS - BLOCK)], r_b.at[c])
+            mine = cotf.at[y, :, lanes(c)]
+            send(mine, mine, s_y.at[0, c], r_yl.at[c], to_right)
+            send(mine, mine, s_y.at[1, c], r_yr.at[c], to_left)
+        c = s - 2
+        if 0 <= c < CH:
+            wait_all(out_b.at[c], r_yl.at[c])
+            passed = cotf.at[left, pl.ds(0, HALF), lanes(c)]
+            send(passed, passed, s_y.at[2, c], r_fl.at[c], to_right)
+            wait_all(out_b.at[c], r_yr.at[c])
+            passed = cotf.at[right, pl.ds(HALF, HALF), lanes(c)]
+            send(passed, passed, s_y.at[3, c], r_fr.at[c], to_left)
+        c = s - 3
+        if 0 <= c < CH:
+            wait_all(out_b.at[c, pl.ds(0, HALF)], r_fl.at[c])
+            wait_all(out_b.at[c, pl.ds(0, HALF)], r_fr.at[c])
+            arrived = jnp.concatenate([cotf[q, :, lanes(c)] for q in range(NY)], axis=1)
+            down = jnp.concatenate(
+                [wd[:, pl.ds(q * WIDE + c * LANES, LANES)] for q in range(NY)], axis=1
+            )
+            term = nt(arrived, down)
+            dact[...] = term if c == 0 else dact[...] + term
+
+    dgu[:, 0:HID] = (dact[...] * f_gate[...]).astype(BF)
+    dgu[:, HID : 2 * HID] = (dact[...] * f_up[...]).astype(BF)
+
+    for c in range(CH):
+        weights = jnp.concatenate(
+            [
+                jnp.concatenate([w[pl.ds(q * WIDE + c * LANES, LANES), :] for w in (wg, wu)], axis=1)
+                for q in range(NY)
+            ],
+            axis=0,
+        )
+        product = nt(dgu[...], weights).astype(BF)
+        for q in range(NY):
+            partial[c, q] = product[:, q * LANES : (q + 1) * LANES]
+        low, high = pl.ds(0, HALF), pl.ds(HALF, HALF)
+        send(partial.at[c, across, low], r1l.at[c], s_rs.at[0, c], r_1l.at[c], to_right)
+        send(partial.at[c, across, high], r1r.at[c], s_rs.at[1, c], r_1r.at[c], to_left)
+        send(partial.at[c, right, high], from_l.at[c, high], s_rs.at[2, c], r_sl.at[c], to_right)
+        send(partial.at[c, left, low], from_r.at[c, low], s_rs.at[3, c], r_sr.at[c], to_left)
+
+    def weight_grads(j):
+        if j < 4:
+            gd_out[:, pl.ds(j * WIDE, WIDE)] = tn(act_s[...], cotf[j]).astype(BF)
+        else:
+            part = pl.ds((j - 4) * 256, 256)
+            both = tn(rows_p[:, part], dgu[...]).astype(BF)
+            gg_out[part, :] = both[:, 0:HID]
+            gu_out[part, :] = both[:, HID : 2 * HID]
+
+    work = 0
+    for s in range(CH + 5):
+        c = s
+        if 0 <= c < CH:
+            low, high = pl.ds(0, HALF), pl.ds(HALF, HALF)
+            wait_all(r1l.at[c], r_1l.at[c])
+            accr[c] = (partial[c, right, low, :].astype(F32) + r1l[c].astype(F32)).astype(BF)
+            send(accr.at[c], from_l.at[c, low], s_rs.at[4, c], r_sl.at[c], to_right)
+            wait_all(r1r.at[c], r_1r.at[c])
+            accl[c] = (partial[c, left, high, :].astype(F32) + r1r[c].astype(F32)).astype(BF)
+            send(accl.at[c], from_r.at[c, high], s_rs.at[5, c], r_sr.at[c], to_left)
+        c = s - 1
+        if 0 <= c < CH:
+            wait_all(from_l.at[c], r_sl.at[c])
+            wait_all(from_r.at[c], r_sr.at[c])
+            total = partial[c, y].astype(F32) + from_l[c].astype(F32) + from_r[c].astype(F32)
+            egrad[c] = total.astype(BF)
+            for step in (4, 2, 6, 3, 5, 1, 7):
+                peer, device = g_peer(step)
+                send(
+                    egrad.at[c, rows_of(peer)], recv_b2.at[c, rows_of(g)],
+                    s_b2.at[c], r_b2.at[c], device,
+                )
+            recv_b2[c, rows_of(g), :] = egrad[c, rows_of(g), :]
+        c = s - 2
+        if 0 <= c < CH:
+            wait_all(recv_b2.at[c, pl.ds(0, ROWS - BLOCK)], r_b2.at[c])
+            out_a2[c] = nn(perm[...], recv_b2[c]).astype(BF)
+            for step in (4, 3, 5, 2, 6, 1, 7):
+                peer, device = z_peer(step)
+                send(
+                    out_a2.at[c, rows_of(peer)], coming.at[c, rows_of(z)],
+                    s_a2.at[c], r_a2.at[c], device,
+                )
+            coming[c, rows_of(z), :] = out_a2[c, rows_of(z), :]
+        c = s - 3
+        if 0 <= c < CH:
+            wait_all(coming.at[c, pl.ds(0, ROWS - BLOCK)], r_a2.at[c])
+            summed = nn(sel_t[...], coming[c])
+            mix[y, :, lanes(c)] = (cot[:, lanes(c)].astype(F32) + summed).astype(BF)
+            mine = mix.at[y, :, lanes(c)]
+            send(mine, mine, s_m.at[0, c], r_ml.at[c], to_right)
+            send(mine, mine, s_m.at[1, c], r_mr.at[c], to_left)
+        c = s - 4
+        if 0 <= c < CH:
+            size = coming.at[c, pl.ds(0, TOK)]
+            wait_all(size, r_ml.at[c])
+            passed = mix.at[left, pl.ds(0, TOK // 2), lanes(c)]
+            send(passed, passed, s_m.at[2, c], r_nl.at[c], to_right)
+            wait_all(size, r_mr.at[c])
+            passed = mix.at[right, pl.ds(TOK // 2, TOK // 2), lanes(c)]
+            send(passed, passed, s_m.at[3, c], r_nr.at[c], to_left)
+        c = s - 5
+        if 0 <= c < CH:
+            size = coming.at[c, pl.ds(0, TOK // 2)]
+            wait_all(size, r_nl.at[c])
+            wait_all(size, r_nr.at[c])
+        for _ in range(2):
+            if work < 12:
+                weight_grads(work)
+                work += 1
+
+    for c in range(CH):
+        full, most, half = out_b.at[c], out_b.at[c, pl.ds(0, ROWS - BLOCK)], out_b.at[c, pl.ds(0, HALF)]
+        for sem in (s_a, s_b, s_b2, s_a2):
+            wait_all(most, sem.at[c])
+        for i, size in enumerate((full, full, half, half)):
+            wait_all(size, s_y.at[i, c])
+        for i in range(6):
+            wait_all(half, s_rs.at[i, c])
+        for i in range(4):
+            wait_all(out_b.at[c, pl.ds(0, TOK if i < 2 else TOK // 2)], s_m.at[i, c])
+
+
+def moe(cot, route_ids, route_weight, rows_in, wg, wu, wd):
+    at = jnp.arange(ROWS, dtype=jnp.int32)
+    swapped = (at // CAP % NZ) * BLOCK + at // BLOCK * CAP + at % CAP
+    perm = (swapped[:, None] == at[None, :]).astype(BF)
+    ids = route_ids.astype(F32)
+    vmem = pl.BlockSpec(memory_space=pltpu.VMEM)
+    dma, V = pltpu.SemaphoreType.DMA, pltpu.VMEM
+    chunked = V((CH, ROWS, LANES), BF)
+    halves = V((CH, HALF, LANES), BF)
+    return pl.pallas_call(
+        moe_kernel,
+        out_shape=(
+            jax.ShapeDtypeStruct((2048, HID), BF),
+            jax.ShapeDtypeStruct((2048, HID), BF),
+            jax.ShapeDtypeStruct((HID, 2048), BF),
+            jax.ShapeDtypeStruct((NY, TOK, WIDE), BF),
+        ),
+        in_specs=[vmem] * 9,
+        out_specs=(vmem,) * 4,
+        scratch_shapes=[
+            chunked, chunked, chunked,
+            V((NY, ROWS, WIDE), BF),
+            V((ROWS, HID), BF), V((ROWS, HID), F32), V((ROWS, HID), F32), V((ROWS, HID), F32),
+            V((ROWS, 2 * HID), BF), V((TOK, ROWS), BF), V((ROWS, 2048), BF),
+            V((CH, NY, ROWS, LANES), BF),
+            halves, halves, halves, halves,
+            chunked, chunked, chunked, chunked, chunked, chunked,
+            dma((CH,)), dma((CH,)), dma((CH,)), dma((CH,)),
+            dma((4, CH)), dma((CH,)), dma((CH,)), dma((CH,)), dma((CH,)),
+            dma((6, CH)), dma((CH,)), dma((CH,)), dma((CH,)), dma((CH,)),
+            dma((CH,)), dma((CH,)), dma((CH,)), dma((CH,)),
+            dma((4, CH)), dma((CH,)), dma((CH,)), dma((CH,)), dma((CH,)),
+        ],
+        compiler_params=pltpu.CompilerParams(
+            collective_id=0, has_side_effects=True, vmem_limit_bytes=60 * 1024 * 1024
+        ),
+        name="moe",
+    )(cot, ids, ids.T, route_weight.T, rows_in, wg, wu, wd, perm)
 
 
 def in_blocks(value, dim, devices):
@@ -83,72 +393,13 @@
     value_pre,
     gate_pre,
 ):
-    group_size = lax.axis_size(SP)
     narrow_size = lax.axis_size("tp")
     tok_rows = cot_out.shape[0]
-    chosen = route_ids.shape[1]
-    slot_rows = expert_inputs.shape[1]
-    capacity = slot_rows // group_size
-    model_width = expert_inputs.shape[2]
     local_cols = cot_out.shape[1]
-    flat_ids = route_ids.reshape(-1)
-    expert_hot = (flat_ids[:, None] == jnp.arange(group_size, dtype=jnp.int32)[None, :]).astype(
-        jnp.int32
-    )
-    earlier = jnp.sum((jnp.cumsum(expert_hot, axis=0) - expert_hot) * expert_hot, axis=1)
-    dest_rows = flat_ids * capacity + earlier
-    flat_weight = route_weight.reshape(-1)[:, None]
-    scaled = (flat_weight * jnp.repeat(cot_out, chosen, axis=0).astype(jnp.float32)).astype(
-        jnp.bfloat16
-    )
-    outgoing = (
-        jnp.zeros((group_size * capacity, local_cols), jnp.bfloat16).at[dest_rows].set(scaled)
-    )
-    moved = lax.all_to_all(
-        outgoing.reshape(group_size, capacity, local_cols),
-        SP,
-        split_axis=0,
-        concat_axis=0,
-        tiled=True,
-    )
-    arrived = lax.all_gather(moved, "tp", axis=2, tiled=True)
-    rows_cot = arrived.reshape(slot_rows, model_width)
-    rows_in = expert_inputs[0]
-    gate_weight = w_gate[0]
-    up_weight = w_up[0]
-    down_weight = w_down[0]
-    gate_lin = jnp.dot(rows_in, gate_weight, preferred_element_type=jnp.float32)
-    up_lin = jnp.dot(rows_in, up_weight, preferred_element_type=jnp.float32)
-    gate_c = jnp.minimum(gate_lin, clamp_limit)
-    up_c = jnp.clip(up_lin, -clamp_limit, clamp_limit)
-    sigma = jax.nn.sigmoid(swish_alpha * gate_c)
-    act = ((up_c + 1.0) * gate_c * sigma).astype(jnp.bfloat16)
-    grad_down = jnp.dot(act.T, rows_cot, preferred_element_type=jnp.float32).astype(jnp.bfloat16)
-    d_act = jnp.dot(rows_cot, down_weight.T, preferred_element_type=jnp.float32)
-    up_open = ((up_lin > -clamp_limit) & (up_lin < clamp_limit)).astype(jnp.float32)
-    gate_open = (gate_lin < clamp_limit).astype(jnp.float32)
-    d_up = (d_act * gate_c * sigma * up_open).astype(jnp.bfloat16)
-    d_gate = (
-        d_act * (up_c + 1.0) * (sigma + swish_alpha * gate_c * sigma * (1.0 - sigma)) * gate_open
-    ).astype(jnp.bfloat16)
-    grad_gate_part = jnp.dot(rows_in.T, d_gate, preferred_element_type=jnp.float32).astype(
-        jnp.bfloat16
-    )
-    grad_up_part = jnp.dot(rows_in.T, d_up, preferred_element_type=jnp.float32).astype(jnp.bfloat16)
-    partial_value = jnp.dot(d_gate, gate_weight.T, preferred_element_type=jnp.float32)
-    partial_value = partial_value + jnp.dot(d_up, up_weight.T, preferred_element_type=jnp.float32)
-    input_grad = sum_at_owner(partial_value.astype(jnp.bfloat16), "tp", 1).astype(jnp.bfloat16)
-    coming = lax.all_to_all(
-        input_grad.reshape(group_size, capacity, local_cols),
-        SP,
-        split_axis=0,
-        concat_axis=0,
-        tiled=True,
-    )
-    picked = coming.reshape(group_size * capacity, local_cols)[dest_rows].astype(jnp.float32)
-    summed = jnp.sum(picked.reshape(tok_rows, chosen, local_cols), axis=1)
-    mix_grad = (cot_out.astype(jnp.float32) + summed).astype(jnp.bfloat16)
-    mix_full = collect(mix_grad, "tp", 1)
+    grad_gate_part, grad_up_part, grad_down, mix = moe(
+        cot_out, route_ids, route_weight, expert_inputs[0], w_gate[0], w_up[0], w_down[0]
+    )
+    mix_full = jnp.transpose(mix, (1, 0, 2)).reshape(tok_rows, -1)
     convolution_filter = conv_out.astype(jnp.float32)
     channel_total = local_cols * narrow_size
     first_sum, square_sum = lax.psum(

time: 354 us -> 245 us (0.69)
  Pallas kernels: 0 us -> 113 us
  blocking collectives: 98.3 us -> 9.95 us
  waiting for transfers between devices: 122 us -> 77 us
  local copies, waits for them, and re-layouts: 38.6 us -> 7.3 us
  matrix products: 28.9 us -> 4.63 us
  other arithmetic: 28.6 us -> 11.4 us
  starting transfers between devices: 20.5 us -> 6.28 us
    pallas_call x0 -> x1, Pallas kernels: none -> 113 us  [moe(): pl.pallas_call(moe_kernel, out_shape=(jax.ShapeDtypeStruct((2048, HID), B...]
    all_to_all x2 -> x0, blocking collectives: 81.9 us -> none  [the longest x1 41 us: sum_at_owner(): lax.all_to_all(tiles, axis, split_axis=0, concat_axis=0, tiled=True)]
    all_gather x1 -> x0, waiting for transfers between devices: 42.5 us -> none  [per_device(): arrived = lax.all_gather(moved, 'tp', axis=2, tiled=True)]
    all_to_all x1 -> x0, waiting for transfers between devices: 28.7 us -> none  [per_device(): lax.all_to_all(input_grad.reshape(group_size, capacity, local_cols), SP,...]
    dot_general x8 -> x0, matrix products: 21.8 us -> none  [the longest x1 4.62 us: per_device(): jnp.dot(act.T, rows_cot, preferred_element_type=jnp.float32)]
    reduce_scatter x3, waiting for transfers between devices: 51 us -> 71.7 us  [sum_by_axis(): subtotal = lax.psum_scatter(subtotal, axis, scatter_dimension=0, tiled=True)]
    reshape x5 -> x0, local copies, waits for them, and re-layouts: 12.7 us -> none  [the longest x1 6.16 us: per_device(): rows_cot = arrived.reshape(slot_rows, model_width)]
    all_to_all x1 -> x0, starting transfers between devices: 10.7 us -> none  [per_device(): lax.all_to_all(input_grad.reshape(group_size, capacity, local_cols), SP,...]
  transfers between devices with their start and end apart: 8 -> 5, of which waited for: 5 -> 4; matrix products, arithmetic and copies ran while one was open for 11% -> 4% of each run, Pallas kernels for 0% -> 0%
where the time goes in v1:
time: 245 us; the launch traced here: 243 us
  Pallas kernels  113 us (46%)
  waiting for transfers between devices  77 us (31%)
  between operations  13.9 us (6%)
  other arithmetic  11.4 us (5%)
  blocking collectives  9.95 us (4%)
  local copies, waits for them, and re-layouts  7.3 us (3%)
  starting transfers between devices  6.28 us (3%)
  matrix products  4.63 us (2%)
    pallas_call x1, Pallas kernels, moe(): pl.pallas_call(moe_kernel, out_shape=(jax.ShapeDtypeStruct((2048, HID), B...  113 us
    reduce_scatter x3, waiting for transfers between devices, sum_by_axis(): subtotal = lax.psum_scatter(subtotal, axis, scatter_dimension=0, tiled=True)  71.7 us
    psum x1, blocking collectives, per_device(): lax.psum((jnp.sum(convolution_filter, axis=1), jnp.sum(convolution_filter...  9.95 us
    all_to_all x1, waiting for transfers between devices, from_everyone(): lax.all_to_all(jnp.broadcast_to(value[None], (devices, *value.shape)), ax...  5.28 us
  transfers between devices with their start and end apart: 5, of which 4 were waited for; matrix products, arithmetic and copies ran while one was open for 4% of the time, Pallas kernels for 0%

profile of v1, /device:TPU:2, one launch (start us, length us, event | category | flops | bytes accessed | tf_op | source)
XLA Modules:
  0.0 242.9 jit_solution(4722588140312494702)
XLA Ops:
  7.2 0.0 copy-start
  7.2 0.0 reduce-scatter.4.cloned.1.call-start
  7.2 1.3 convert_reduce_fusion
  8.5 1.3 convert_bitcast_fusion
  9.8 0.8 copy.24.ids_c
  10.6 1.3 fusion.perm
  11.8 112.5 %moe.1 = (bf16[2048,256]{1,0:T(8,128)(2,1)}, bf16[2048,256]{1,0:T(8,128)(2,1)}, bf16[256,2048]{1,0:T(8,128)(2,1)}, bf16[4,256,512]{2,1,0:T(8,128)(2,1)}) custom-call(bf16[256,512]{1,0:T(8,128)(2,1)} %cot.1, f32[256,2]{1,0:T(8,128)} %copy.24.ids_c, f32[2,256]{1,0:T(2,128)} %get-tuple-element.55.ids_r, f32[2,256]{1,0:T(2,128)} %bitcast.87, ...), custom_call_target="tpu_custom_call" | custom-call | tf_op jit(solution)/shard_map/moe/pallas_call | solution.py:295
  124.4 0.0 copy-start.1
  124.4 0.0 copy-start.5
  124.4 1.5 copy.25
  125.9 10.0 %all-reduce = (f32[256]{0:T(256)S(1)}, f32[256]{0:T(256)S(1)}) all-reduce(f32[256]{0:T(256)S(1)} %get-tuple-element.17, f32[256]{0:T(256)S(1)} %get-tuple-element.16), channel_id=1, replica_groups=mesh['sp_0'=8,'sp_1'=4,'sp_2'=2,'tp'=4] {'tp'}, use_global_device_ids=true, to_apply=%region_3.4 | all-reduce | flops 512 | bytes 4096 | tf_op jit(solution)/shard_map/psum | solution.py:405
  135.9 0.0 copy-done.1
  135.9 0.0 copy-done.5
  135.9 2.9 %fusion.108 = f32[512,2048]{1,0:T(8,128)} fusion(bf16[256,2048]{0,1:T(8,128)(2,1)S(1)} %bitcast.46, bf16[256,512]{1,0:T(8,128)(2,1)S(1)} %copy-done.1, f32[512]{0:T(512)S(1)} %copy-done.5, f32[256]{0:T(256)S(1)} %get-tuple-element.58, f32[256]{0:T(256)S(1)} %get-tuple-element.57), kind=kOutput, calls=%fused_computation.175 | convolution fusion | flops 538050560 | bytes 5509120 | tf_op jit(solution)/shard_map/dot_general | solution.py:420
  138.8 0.0 reduce-scatter.4.cloned.1.call-update
  138.8 0.0 reduce-scatter.6.cloned.1.call-start
  138.8 52.2 %reduce-scatter.4.cloned.1.call-done = f32[64,2048]{1,0:T(8,128)} async-done(((f32[512,2048]{1,0:T(8,128)}), f32[64,2048]{1,0:T(8,128)}) %reduce-scatter.4.cloned.1.call-update) | async-done | bytes 524304 | tf_op jit(solution)/shard_map/reduce_scatter | solution.py:358
  191.0 0.0 reduce-scatter.6.cloned.1.call-update
  191.0 0.0 copy-done
  191.0 0.0 copy-start.4
  191.1 1.7 fusion.129
  192.8 0.6 broadcast_in_dim.11
  193.4 4.3 %all-to-all-start = ((f32[4,1,512]{2,1,0:T(1,128)}), f32[4,1,512]{2,1,0:T(1,128)S(1)}, u32[]{:S(2)}, u32[]{:S(2)}) async-start(f32[4,1,512]{2,1,0:T(1,128)} %broadcast_in_dim.11), calls=%async_computation.3 | async-start | bytes 16384 | tf_op jit(solution)/shard_map/all_to_all | solution.py:340
  197.7 0.0 reduce-scatter.8.cloned.1.call-start
  197.7 0.0 copy-done.4
  197.7 5.3 %all-to-all-done = f32[4,1,512]{2,1,0:T(1,128)S(1)} async-done(((f32[4,1,512]{2,1,0:T(1,128)}), f32[4,1,512]{2,1,0:T(1,128)S(1)}, u32[]{:S(2)}, u32[]{:S(2)}) %all-to-all-start) | async-done | bytes 8224 | tf_op jit(solution)/shard_map/all_to_all | solution.py:340
  203.0 1.3 fusion.105
  204.3 1.9 collective-permute-start
  206.3 8.1 %reduce-scatter.6.cloned.1.call-done = f32[16,2048]{1,0:T(8,128)} async-done(((f32[64,2048]{1,0:T(8,128)}), f32[16,2048]{1,0:T(8,128)}) %reduce-scatter.6.cloned.1.call-update) | async-done | bytes 131088 | tf_op jit(solution)/shard_map/reduce_scatter | solution.py:358
  214.3 0.0 reduce-scatter.8.cloned.1.call-update
  214.4 0.0 collective-permute-done
  214.4 4.4 %multiply_convert_fusion = (bf16[256,512]{1,0:T(8,128)(2,1)}, f32[256,512]{1,0:T(8,128)S(1)}) fusion(bf16[256,512]{1,0:T(8,128)(2,1)} %param.24, bf16[256,512]{1,0:T(8,128)(2,1)} %param.25, f32[256,512]{1,0:T(8,128)S(1)} %fusion.105, f32[512]{0:T(512)S(1)} %bitcast.85, f32[30,512]{1,0:T(8,128)S(1)} %collective-permute-done, f32[512]{0:T(512)S(1)} %bitcast.86, ...), kind=kLoop, calls=%fused_computation.172 | loop fusion | flops 13238272 | bytes 1959936 | tf_op jit(solution)/shard_map/convert_element_type | solution.py:453
  218.7 0.0 copy-start.3
  218.8 1.9 multiply_convert_fusion.1
  220.6 11.5 %reduce-scatter.8.cloned.1.call-done = f32[8,2048]{1,0:T(8,128)} async-done(((f32[16,2048]{1,0:T(8,128)}), f32[8,2048]{1,0:T(8,128)}) %reduce-scatter.8.cloned.1.call-update) | async-done | bytes 65552 | tf_op jit(solution)/shard_map/reduce_scatter | solution.py:358
  232.1 0.0 copy-start.2
  232.1 2.4 copy.33
  234.5 0.0 copy-done.3
  234.5 1.0 copy.34
  235.4 0.0 copy-done.2
  235.4 1.0 copy.35
  (8 shorter events, 0.1 us)
Async XLA Ops:
  7.2 183.9 %copy-start = (bf16[512,2048]{1,0:T(8,128)(2,1)S(1)}, bf16[512,2048]{1,0:T(8,128)(2,1)}, u32[]{:S(2)}) copy-start(bf16[512,2048]{1,0:T(8,128)(2,1)} %param.20) | copy-start | bytes 6291460
  7.2 183.8 %reduce-scatter.4.cloned.1.call-start = ((), (), s32[]{:S(2)}) async-start(), calls=%async_computation.4 | async-start | bytes 4718592 | tf_op jit(solution)/shard_map/reduce_scatter | solution.py:358
  124.4 11.5 %copy-start.1 = (bf16[256,512]{1,0:T(8,128)(2,1)S(1)}, bf16[256,512]{1,0:T(8,128)(2,1)}, u32[]{:S(2)}) copy-start(bf16[256,512]{1,0:T(8,128)(2,1)} %param.21) | copy-start | bytes 786436
  124.4 11.5 %copy-start.5 = (f32[512]{0:T(512)S(1)}, f32[512]{0:T(512)}, u32[]{:S(2)}) copy-start(f32[512]{0:T(512)} %param.22) | copy-start | bytes 6148
  138.8 75.5 %reduce-scatter.6.cloned.1.call-start = ((), (), s32[]{:S(2)}) async-start(), calls=%async_computation.5 | async-start | bytes 655360 | tf_op jit(solution)/shard_map/reduce_scatter | solution.py:358
  191.0 6.6 %copy-start.4 = (f32[31,512]{1,0:T(8,128)S(1)}, f32[31,512]{1,0:T(8,128)}, u32[]{:S(2)}) copy-start(f32[31,512]{1,0:T(8,128)} %param.23) | copy-start | bytes 190468
  193.4 9.6 %all-to-all-start = ((f32[4,1,512]{2,1,0:T(1,128)}), f32[4,1,512]{2,1,0:T(1,128)S(1)}, u32[]{:S(2)}, u32[]{:S(2)}) async-start(f32[4,1,512]{2,1,0:T(1,128)} %broadcast_in_dim.11), calls=%async_computation.3 | async-start | bytes 16384 | tf_op jit(solution)/shard_map/all_to_all | solution.py:340
  197.7 34.4 %reduce-scatter.8.cloned.1.call-start = ((), (), s32[]{:S(2)}) async-start(), calls=%async_computation.6 | async-start | bytes 196608 | tf_op jit(solution)/shard_map/reduce_scatter | solution.py:358
  204.3 10.0 %collective-permute-start = (f32[30,512]{1,0:T(8,128)S(1)}, f32[30,512]{1,0:T(8,128)S(1)}, u32[]{:S(2)}, u32[]{:S(2)}) collective-permute-start(f32[30,512]{1,0:T(8,128)S(1)} %slice.256), channel_id=1, source_target_pairs={{4,0},{8,4},{12,8},{16,12},{20,16},{24,20},{28,24},{32,28},{36,32}... | collective-permute-start | bytes 184328 | tf_op jit(solution)/shard_map/ppermute | solution.py:378
  218.7 15.7 %copy-start.3 = (bf16[2048,256]{1,0:T(8,128)(2,1)S(1)}, bf16[2048,256]{1,0:T(8,128)(2,1)}, u32[]{:S(2)}) copy-start(bf16[2048,256]{1,0:T(8,128)(2,1)} %get-tuple-element.11) | copy-start | bytes 3145732
  232.1 3.3 %copy-start.2 = (bf16[256,2048]{1,0:T(8,128)(2,1)S(1)}, bf16[256,2048]{1,0:T(8,128)(2,1)}, u32[]{:S(2)}) copy-start(bf16[256,2048]{1,0:T(8,128)(2,1)} %get-tuple-element.12) | copy-start | bytes 3145732
Sparse Core Ops, SparseCore 0:
  138.9 52.0 reduce-scatter.3
  193.5 20.7 reduce-scatter.5
  217.4 14.6 reduce-scatter.7

commit v2 on v1

v2 whole, which is shorter than its diff:
```python
import jax
import jax.numpy as jnp
from jax import lax
from jax.experimental import pallas as pl
from jax.experimental.pallas import tpu as pltpu
from jax.sharding import Mesh
from jax.sharding import PartitionSpec as P

SP = ("sp_0", "sp_1", "sp_2")
TP_SP = ("tp", "sp_0", "sp_1", "sp_2")
MESH = pl.DeviceIdType.MESH

clamp_limit = 7.0
swish_alpha = 1.702
norm_epsilon = 1e-05

CH = 4
LANES = 128
NZ = 8
NG = 8
NY = 4
CAP = 12
BLOCK = NZ * CAP
ROWS = NZ * BLOCK
HALF = ROWS // 2
TOK = 256
WIDE = CH * LANES
HID = 256
TAPS = 31
EXT = TOK + 32
CHANNELS = 2048
NX = 4
XROWS = 64
BF = jnp.bfloat16
F32 = jnp.float32


def nt(a, b):
    return lax.dot_general(a, b, (((1,), (1,)), ((), ())), preferred_element_type=F32)


def tn(a, b):
    return lax.dot_general(a, b, (((0,), (0,)), ((), ())), preferred_element_type=F32)


def nn(a, b):
    return lax.dot_general(a, b, (((1,), (0,)), ((), ())), preferred_element_type=F32)


def wait_all(ref, sem):
    pltpu.make_async_copy(ref, ref, sem).wait()


def send(src, dst, send_sem, recv_sem, device):
    pltpu.make_async_remote_copy(
        src_ref=src,
        dst_ref=dst,
        send_sem=send_sem,
        recv_sem=recv_sem,
        device_id=device,
        device_id_type=MESH,
    ).start()


def lanes(c):
    return pl.ds(c * LANES, LANES)


def rows_of(block):
    return pl.ds(pl.multiple_of(block * BLOCK, BLOCK), BLOCK)


def columns(parts, rows):
    lane = lax.broadcasted_iota(jnp.int32, (rows, LANES), 1)
    whole = jnp.zeros((rows, LANES), F32)
    for i, part in enumerate(parts):
        whole = jnp.where(lane == i, part, whole)
    return whole


def as_columns(rows8):
    return jnp.concatenate([rows8, jnp.zeros((LANES - 8, TOK), F32)], axis=0).T


def swap_matrix():
    at = lax.broadcasted_iota(jnp.int32, (ROWS, 1), 0).astype(F32)
    pair = jnp.floor((at + 0.5) * (1.0 / CAP))
    high = jnp.floor((pair + 0.5) * (1.0 / NZ))
    source = (pair - NZ * high) * BLOCK + high * CAP + (at - CAP * pair)
    lane = lax.broadcasted_iota(jnp.int32, (ROWS, ROWS), 1).astype(F32)
    return jnp.where(lane == source, 1.0, 0.0).astype(BF)


def step_kernel(
    cot, ids, route_w, conv, gain, taps, rows_hbm, wg_hbm, wu_hbm, wd_hbm, wp_hbm, value_hbm, gate_hbm,
    gg_hbm, gu_hbm, gd_hbm, gp_out, gv_out, gt_out,
    rows_in, wg, wu, wd, wp, value, gate, gg_out, gu_out, gd_out,
    perm, out_a, recv_a, out_b, cotf, act_s, f_up, f_gate, dact, dgu, sel_t, rows_p,
    partial, r1l, r1r, accl, accr, from_l, from_r, egrad, recv_b2, out_a2, coming, mix,
    stat, nstat, xhat, act_c, fac, rstd_s, sg, vg, dac, ext, halo,
    gpb, rc, gx, x1l, x1r, xal, xar, xfl, xfr, gz, rz,
    s_in, s_out,
    s_a, r_a, s_b, r_b, s_y, r_yl, r_yr, r_fl, r_fr,
    s_rs, r_1l, r_1r, r_sl, r_sr, s_b2, r_b2, s_a2, r_a2, s_m, r_ml, r_mr, r_nl, r_nr,
    s_stat, r_stat, s_n, r_n, s_h, r_h,
    s_c, r_c, s_x, r_x1l, r_x1r, r_xl, r_xr, s_z, r_z,
):
    z = lax.axis_index("sp_0")
    x = lax.axis_index("sp_1")
    core = lax.axis_index("sp_2")
    g = x * 2 + core
    y = lax.axis_index("tp")
    right, left, across = lax.rem(y + 1, NY), lax.rem(y + 3, NY), lax.rem(y + 2, NY)
    to_right, to_left, to_across = {"tp": right}, {"tp": left}, {"tp": across}
    x_right, x_left, x_across = lax.rem(x + 1, NX), lax.rem(x + 3, NX), lax.rem(x + 2, NX)
    to_x_right, to_x_left = {"sp_1": x_right}, {"sp_1": x_left}
    to_core = {"sp_2": 1 - core}
    place = z * NG + g

    def z_peer(step):
        peer = lax.rem(z + step, NZ)
        return peer, {"sp_0": peer}

    def g_peer(step):
        peer = lax.rem(g + step, NG)
        return peer, {"sp_1": peer // 2, "sp_2": lax.rem(peer, 2)}

    def in_line(step):
        other = lax.rem(place + step, NZ * NG)
        return {"sp_0": other // NG, "sp_1": lax.rem(other // 2, NX), "sp_2": lax.rem(other, 2)}

    to_before = in_line(NZ * NG - 1)
    barrier = pltpu.get_barrier_semaphore()
    greeted = [z_peer(step)[1] for step in range(1, NZ)] + [g_peer(step)[1] for step in range(1, NG)]
    greeted += [to_right, to_left, to_across, to_before, in_line(1)]
    for device in greeted:
        pl.semaphore_signal(barrier, inc=1, device_id=device, device_id_type=MESH)

    fetches = [
        pltpu.make_async_copy(src, dst, s_in.at[i])
        for i, (src, dst) in enumerate(
            ((rows_hbm, rows_in), (wg_hbm, wg), (wu_hbm, wu), (wd_hbm, wd),
             (gate_hbm, gate), (value_hbm, value), (wp_hbm, wp))
        )
    ]
    for fetch in fetches:
        fetch.start()

    t_sub = lax.broadcasted_iota(jnp.int32, (TOK, TOK), 0)
    t_lane = lax.broadcasted_iota(jnp.int32, (TOK, TOK), 1)
    before, after = t_sub < t_lane, t_lane < t_sub
    col = [ids[:, k : k + 1].astype(F32) for k in (0, 1)]
    turned = columns(col + [route_w[:, k : k + 1] for k in (0, 1)], TOK).T
    row = [turned[k : k + 1, :] for k in (0, 1)]
    w_r = [turned[k + 2 : k + 3, :] for k in (0, 1)]
    slot_r = lax.broadcasted_iota(jnp.int32, (ROWS, TOK), 0).astype(F32)
    chosen, weight = None, None
    for k in (0, 1):
        same = ((col[0] == row[k]) | (col[1] == row[k])) & before
        dest = jnp.sum(jnp.where(same, 1.0, 0.0), axis=0, keepdims=True) + CAP * row[k]
        hot = slot_r == dest
        one, scale = jnp.where(hot, 1.0, 0.0), jnp.where(hot, w_r[k], 0.0)
        chosen = one if chosen is None else chosen + one
        weight = scale if weight is None else weight + scale
    chosen = chosen.astype(BF)
    weight = jnp.sum(weight, axis=1, keepdims=True)

    for c in range(CH):
        out_a[c] = (weight * nn(chosen, cot[:, lanes(c)])).astype(BF)
        if c == 0:
            pl.semaphore_wait(barrier, len(greeted))
        for step in (4, 3, 5, 2, 6, 1, 7):
            peer, device = z_peer(step)
            send(out_a.at[c, rows_of(peer)], recv_a.at[c, rows_of(z)], s_a.at[c], r_a.at[c], device)
        recv_a[c, rows_of(z), :] = out_a[c, rows_of(z), :]

    wide = conv[...].astype(F32)
    sums = [jnp.sum(v, axis=1, keepdims=True) for v in (wide, wide * wide)]
    stat[y] = columns(sums, TOK).T[0:8, :]
    for i, device in enumerate((to_right, to_left, to_across)):
        send(stat.at[y], stat.at[y], s_stat.at[i], r_stat.at[0], device)

    perm[...] = swap_matrix()

    def unpack_slots():
        slot_c = lax.broadcasted_iota(jnp.int32, (TOK, ROWS), 1).astype(F32)
        back = None
        for k in (0, 1):
            same = ((row[0] == col[k]) | (row[1] == col[k])) & after
            dest = jnp.sum(jnp.where(same, 1.0, 0.0), axis=1, keepdims=True) + CAP * col[k]
            one = jnp.where(slot_c == dest, 1.0, 0.0)
            back = one if back is None else back + one
        sel_t[...] = back.astype(BF)

    def forward_rows():
        fetches[0].wait()
        for j in range(8):
            cols = pl.ds(j * 256, 256)
            rows_p[:, cols] = nn(perm[...], rows_in[:, cols]).astype(BF)
        fetches[1].wait()
        fetches[2].wait()
        fetches[3].wait()

    def forward_part(j):
        part = pl.ds(j * 256, 256)
        gate_lin = nn(rows_p[part, :], wg[...])
        up_lin = nn(rows_p[part, :], wu[...])
        gate_c = jnp.minimum(gate_lin, clamp_limit)
        up_c = jnp.clip(up_lin, -clamp_limit, clamp_limit)
        sig = jax.nn.sigmoid(swish_alpha * gate_c)
        act_s[part, :] = ((up_c + 1.0) * gate_c * sig).astype(BF)
        up_open = (up_lin > -clamp_limit) & (up_lin < clamp_limit)
        f_up[part, :] = jnp.where(up_open, gate_c * sig, 0.0)
        slope = (up_c + 1.0) * (sig + swish_alpha * gate_c * sig * (1.0 - sig))
        f_gate[part, :] = jnp.where(gate_lin < clamp_limit, slope, 0.0)

    def norm_terms():
        wait_all(stat.at[pl.ds(0, NY - 1)], r_stat.at[0])
        total = as_columns(stat[0] + stat[1] + stat[2] + stat[3])
        mean = total[:, 0:1] / CHANNELS
        var = total[:, 1:2] / CHANNELS - mean * mean
        rstd = lax.rsqrt(var + norm_epsilon)
        rstd_s[...] = rstd
        normalized = (conv[...].astype(F32) - mean) * rstd
        xhat[...] = normalized
        normed = normalized * gain[...]
        s = jax.nn.sigmoid(normed)
        act_c[...] = (normed * s).astype(BF)
        fac[...] = s * (1.0 + normed * (1.0 - s)) * gain[...]

    def glu_terms():
        fetches[4].wait()
        fetches[5].wait()
        gate_sig = jax.nn.sigmoid(gate[...].astype(F32))
        sg[...] = gate_sig
        vg[...] = value[...].astype(F32) * gate_sig * (1.0 - gate_sig)
        fetches[6].wait()

    fill = [unpack_slots, norm_terms, glu_terms]
    forward_rows()
    for j in range(3):
        forward_part(j)

    for s in range(CH + 3):
        c = s
        if 0 <= c < CH:
            wait_all(recv_a.at[c, pl.ds(0, ROWS - BLOCK)], r_a.at[c])
            out_b[c] = nn(perm[...], recv_a[c]).astype(BF)
            for step in (4, 2, 6, 3, 5, 1, 7):
                peer, device = g_peer(step)
                send(
                    out_b.at[c, rows_of(peer)], cotf.at[y, rows_of(g), lanes(c)],
                    s_b.at[c], r_b.at[c], device,
                )
            cotf[y, rows_of(g), lanes(c)] = out_b[c, rows_of(g), :]
        c = s - 1
        if 0 <= c < CH:
            wait_all(out_b.at[c, pl.ds(0, ROWS - BLOCK)], r_b.at[c])
            mine = cotf.at[y, :, lanes(c)]
            send(mine, mine, s_y.at[0, c], r_yl.at[c], to_right)
            send(mine, mine, s_y.at[1, c], r_yr.at[c], to_left)
        c = s - 2
        if 0 <= c < CH:
            wait_all(out_b.at[c], r_yl.at[c])
            passed = cotf.at[left, pl.ds(0, HALF), lanes(c)]
            send(passed, passed, s_y.at[2, c], r_fl.at[c], to_right)
            wait_all(out_b.at[c], r_yr.at[c])
            passed = cotf.at[right, pl.ds(HALF, HALF), lanes(c)]
            send(passed, passed, s_y.at[3, c], r_fr.at[c], to_left)
        c = s - 3
        if 0 <= c < CH:
            wait_all(out_b.at[c, pl.ds(0, HALF)], r_fl.at[c])
            wait_all(out_b.at[c, pl.ds(0, HALF)], r_fr.at[c])
            arrived = jnp.concatenate([cotf[q, :, lanes(c)] for q in range(NY)], axis=1)
            down = jnp.concatenate(
                [wd[:, pl.ds(q * WIDE + c * LANES, LANES)] for q in range(NY)], axis=1
            )
            term = nt(arrived, down)
            dact[...] = term if c == 0 else dact[...] + term
        if fill:
            fill.pop(0)()

    dgu[:, 0:HID] = (dact[...] * f_gate[...]).astype(BF)
    dgu[:, HID : 2 * HID] = (dact[...] * f_up[...]).astype(BF)

    for c in range(CH):
        weights = jnp.concatenate(
            [
                jnp.concatenate([w[pl.ds(q * WIDE + c * LANES, LANES), :] for w in (wg, wu)], axis=1)
                for q in range(NY)
            ],
            axis=0,
        )
        product = nt(dgu[...], weights).astype(BF)
        for q in range(NY):
            partial[c, q] = product[:, q * LANES : (q + 1) * LANES]
        low, high = pl.ds(0, HALF), pl.ds(HALF, HALF)
        send(partial.at[c, across, low], r1l.at[c], s_rs.at[0, c], r_1l.at[c], to_right)
        send(partial.at[c, across, high], r1r.at[c], s_rs.at[1, c], r_1r.at[c], to_left)
        send(partial.at[c, right, high], from_l.at[c, high], s_rs.at[2, c], r_sl.at[c], to_right)
        send(partial.at[c, left, low], from_r.at[c, low], s_rs.at[3, c], r_sr.at[c], to_left)

    def weight_grads(j):
        if j < 4:
            gd_out[:, pl.ds(j * WIDE, WIDE)] = tn(act_s[...], cotf[j]).astype(BF)
        else:
            part = pl.ds((j - 4) * 256, 256)
            both = tn(rows_p[:, part], dgu[...]).astype(BF)
            gg_out[part, :] = both[:, 0:HID]
            gu_out[part, :] = both[:, HID : 2 * HID]

    stores = [
        pltpu.make_async_copy(src, dst, s_out.at[i])
        for i, (src, dst) in enumerate(((gg_out, gg_hbm), (gu_out, gu_hbm), (gd_out, gd_hbm)))
    ]

    def norm_grad_sums():
        grad = dac[...] * fac[...]
        dac[...] = grad
        sums = [jnp.sum(v, axis=1, keepdims=True) for v in (grad, grad * xhat[...])]
        nstat[y] = columns(sums, TOK).T[0:8, :]
        for i, device in enumerate((to_right, to_left, to_across)):
            send(nstat.at[y], nstat.at[y], s_n.at[i], r_n.at[0], device)

    def conv_grad():
        wait_all(nstat.at[pl.ds(0, NY - 1)], r_n.at[0])
        total = as_columns(nstat[0] + nstat[1] + nstat[2] + nstat[3]) / CHANNELS
        ext[0:TOK, :] = rstd_s[...] * (dac[...] - total[:, 0:1] - xhat[...] * total[:, 1:2])
        send(ext.at[pl.ds(0, 32)], halo, s_h.at[0], r_h.at[0], to_before)

    def conv_rows(begin):
        part = pl.ds(begin, TOK // 2)

        def column(j, carry):
            cols = pl.ds(pl.multiple_of(j * LANES, LANES), LANES)
            total = jnp.zeros((TOK // 2, LANES), F32)
            for k in range(TAPS):
                total = total + taps[k : k + 1, cols] * ext[pl.ds(begin + TAPS - 1 - k, TOK // 2), cols]
            gv_out[part, cols] = (total * sg[part, cols]).astype(BF)
            gt_out[part, cols] = (total * vg[part, cols]).astype(BF)
            return carry

        lax.fori_loop(0, CH, column, 0)

    def conv_first():
        conv_rows(0)

    def conv_rest():
        wait_all(halo, r_h.at[0])
        keep = jnp.where(place == NZ * NG - 1, 0.0, 1.0)
        ext[TOK:EXT, :] = halo[...] * keep
        conv_rows(TOK // 2)

    work = 0
    for s in range(CH + 9):
        c = s
        if 0 <= c < CH:
            low, high = pl.ds(0, HALF), pl.ds(HALF, HALF)
            wait_all(r1l.at[c], r_1l.at[c])
            accr[c] = (partial[c, right, low, :].astype(F32) + r1l[c].astype(F32)).astype(BF)
            send(accr.at[c], from_l.at[c, low], s_rs.at[4, c], r_sl.at[c], to_right)
            wait_all(r1r.at[c], r_1r.at[c])
            accl[c] = (partial[c, left, high, :].astype(F32) + r1r[c].astype(F32)).astype(BF)
            send(accl.at[c], from_r.at[c, high], s_rs.at[5, c], r_sr.at[c], to_left)
        c = s - 1
        if 0 <= c < CH:
            wait_all(from_l.at[c], r_sl.at[c])
            wait_all(from_r.at[c], r_sr.at[c])
            total = partial[c, y].astype(F32) + from_l[c].astype(F32) + from_r[c].astype(F32)
            egrad[c] = total.astype(BF)
            for step in (4, 2, 6, 3, 5, 1, 7):
                peer, device = g_peer(step)
                send(
                    egrad.at[c, rows_of(peer)], recv_b2.at[c, rows_of(g)],
                    s_b2.at[c], r_b2.at[c], device,
                )
            recv_b2[c, rows_of(g), :] = egrad[c, rows_of(g), :]
        c = s - 2
        if 0 <= c < CH:
            wait_all(recv_b2.at[c, pl.ds(0, ROWS - BLOCK)], r_b2.at[c])
            out_a2[c] = nn(perm[...], recv_b2[c]).astype(BF)
            for step in (4, 3, 5, 2, 6, 1, 7):
                peer, device = z_peer(step)
                send(
                    out_a2.at[c, rows_of(peer)], coming.at[c, rows_of(z)],
                    s_a2.at[c], r_a2.at[c], device,
                )
            coming[c, rows_of(z), :] = out_a2[c, rows_of(z), :]
        c = s - 3
        if 0 <= c < CH:
            wait_all(coming.at[c, pl.ds(0, ROWS - BLOCK)], r_a2.at[c])
            summed = nn(sel_t[...], coming[c])
            mix[y, :, lanes(c)] = (cot[:, lanes(c)].astype(F32) + summed).astype(BF)
            mine = mix.at[y, :, lanes(c)]
            send(mine, mine, s_m.at[0, c], r_ml.at[c], to_right)
            send(mine, mine, s_m.at[1, c], r_mr.at[c], to_left)
        c = s - 4
        if 0 <= c < CH:
            size = coming.at[c, pl.ds(0, TOK)]
            wait_all(size, r_ml.at[c])
            passed = mix.at[left, pl.ds(0, TOK // 2), lanes(c)]
            send(passed, passed, s_m.at[2, c], r_nl.at[c], to_right)
            wait_all(size, r_mr.at[c])
            passed = mix.at[right, pl.ds(TOK // 2, TOK // 2), lanes(c)]
            send(passed, passed, s_m.at[3, c], r_nr.at[c], to_left)
        c = s - 5
        if 0 <= c < CH:
            size = coming.at[c, pl.ds(0, TOK // 2)]
            wait_all(size, r_nl.at[c])
            wait_all(size, r_nr.at[c])
            arrived = jnp.concatenate([mix[q, :, lanes(c)] for q in range(NY)], axis=1)
            proj = jnp.concatenate(
                [wp[:, pl.ds(q * WIDE + c * LANES, LANES)] for q in range(NY)], axis=1
            )
            term = nt(arrived, proj)
            dac[...] = term if c == 0 else dac[...] + term
            if c == CH - 1:
                norm_grad_sums()
            product = tn(act_c[...], arrived)
            for core_at in range(2):
                for x_at in range(NX):
                    gpb[c, core_at, x_at] = jnp.concatenate(
                        [
                            product[(z_at * NG + x_at * 2 + core_at) * 8 :][:8]
                            for z_at in range(NZ)
                        ],
                        axis=0,
                    ).astype(BF)
            send(gpb.at[c, 1 - core], rc.at[c], s_c.at[c], r_c.at[c], to_core)
        c = s - 6
        if 0 <= c < CH:
            wait_all(rc.at[c], r_c.at[c])
            gx[c] = (gpb[c, core].astype(F32) + rc[c].astype(F32)).astype(BF)
            low, high = pl.ds(0, XROWS // 2), pl.ds(XROWS // 2, XROWS // 2)
            send(gx.at[c, x_across, low], x1l.at[c], s_x.at[0, c], r_x1l.at[c], to_x_right)
            send(gx.at[c, x_across, high], x1r.at[c], s_x.at[1, c], r_x1r.at[c], to_x_left)
            send(gx.at[c, x_right, high], xfl.at[c, high], s_x.at[2, c], r_xl.at[c], to_x_right)
            send(gx.at[c, x_left, low], xfr.at[c, low], s_x.at[3, c], r_xr.at[c], to_x_left)
        c = s - 7
        if 0 <= c < CH:
            low, high = pl.ds(0, XROWS // 2), pl.ds(XROWS // 2, XROWS // 2)
            wait_all(x1l.at[c], r_x1l.at[c])
            xar[c] = (gx[c, x_right, low, :].astype(F32) + x1l[c].astype(F32)).astype(BF)
            send(xar.at[c], xfl.at[c, low], s_x.at[4, c], r_xl.at[c], to_x_right)
            wait_all(x1r.at[c], r_x1r.at[c])
            xal[c] = (gx[c, x_left, high, :].astype(F32) + x1r[c].astype(F32)).astype(BF)
            send(xal.at[c], xfr.at[c, high], s_x.at[5, c], r_xr.at[c], to_x_left)
            if c == CH - 2:
                conv_grad()
        c = s - 8
        if 0 <= c < CH:
            wait_all(xfl.at[c], r_xl.at[c])
            wait_all(xfr.at[c], r_xr.at[c])
            total = gx[c, x].astype(F32) + xfl[c].astype(F32) + xfr[c].astype(F32)
            gz[c] = jnp.concatenate(
                [
                    total[z_at * 8 : z_at * 8 + 8, half * 256 : half * 256 + 256]
                    for z_at in range(NZ)
                    for half in (0, 1)
                ],
                axis=0,
            ).astype(BF)
            for step in (4, 3, 5, 2, 6, 1, 7):
                peer, device = z_peer(step)
                send(
                    gz.at[c, pl.ds(pl.multiple_of(peer * 16, 16), 16)],
                    rz.at[c, pl.ds(pl.multiple_of(z * 16, 16), 16)],
                    s_z.at[c], r_z.at[c], device,
                )
            own = pl.ds(pl.multiple_of(z * 16, 16), 16)
            rz[c, own, :] = gz[c, own, :]
            if c == CH - 2:
                conv_first()
            if c == CH - 1:
                conv_rest()
        for _ in range(2):
            if work < 12:
                weight_grads(work)
                work += 1
                if work == 4:
                    stores[2].start()
                if work == 12:
                    stores[0].start()
                    stores[1].start()

    for c in range(CH):
        wait_all(rz.at[c, pl.ds(0, 112)], r_z.at[c])
        total = rz[c, 0:16, :].astype(F32)
        for z_at in range(1, NZ):
            total = total + rz[c, z_at * 16 : z_at * 16 + 16, :].astype(F32)
        for q in range(NY):
            row_at, lane_at = (q // 2) * 8, (q % 2) * LANES
            gp_out[:, pl.ds(q * WIDE + c * LANES, LANES)] = total[
                row_at : row_at + 8, lane_at : lane_at + LANES
            ]

    for c in range(CH):
        full, most, half = out_b.at[c], out_b.at[c, pl.ds(0, ROWS - BLOCK)], out_b.at[c, pl.ds(0, HALF)]
        for sem in (s_a, s_b, s_b2, s_a2):
            wait_all(most, sem.at[c])
        for i, size in enumerate((full, full, half, half)):
            wait_all(size, s_y.at[i, c])
        for i in range(6):
            wait_all(half, s_rs.at[i, c])
        for i in range(4):
            wait_all(out_b.at[c, pl.ds(0, TOK if i < 2 else TOK // 2)], s_m.at[i, c])
        wait_all(rc.at[c], s_c.at[c])
        for i in range(6):
            wait_all(x1l.at[c], s_x.at[i, c])
        wait_all(rz.at[c, pl.ds(0, 112)], s_z.at[c])
    for i in range(3):
        wait_all(stat.at[0], s_stat.at[i])
        wait_all(nstat.at[0], s_n.at[i])
        stores[i].wait()
    wait_all(halo, s_h.at[0])


def per_device(
    cot_out,
    route_ids,
    route_weight,
    expert_inputs,
    w_gate,
    w_up,
    w_down,
    w_proj,
    conv_out,
    channel_norm_gain,
    taps,
    value_pre,
    gate_pre,
):
    vmem = pl.BlockSpec(memory_space=pltpu.VMEM)
    anywhere = pl.BlockSpec(memory_space=pl.ANY)
    dma, V = pltpu.SemaphoreType.DMA, pltpu.VMEM
    chunked = V((CH, ROWS, LANES), BF)
    halves = V((CH, HALF, LANES), BF)
    tokens = V((TOK, WIDE), F32)
    x_half = V((CH, XROWS // 2, WIDE), BF)
    per_chunk = dma((CH,))
    gate_grad, up_grad, down_grad, proj_grad, grad_value, grad_gate = pl.pallas_call(
        step_kernel,
        out_shape=(
            jax.ShapeDtypeStruct((CHANNELS, HID), BF),
            jax.ShapeDtypeStruct((CHANNELS, HID), BF),
            jax.ShapeDtypeStruct((HID, CHANNELS), BF),
            jax.ShapeDtypeStruct((8, CHANNELS), F32),
            jax.ShapeDtypeStruct((TOK, WIDE), BF),
            jax.ShapeDtypeStruct((TOK, WIDE), BF),
        ),
        in_specs=[vmem] * 6 + [anywhere] * 7,
        out_specs=(anywhere,) * 3 + (vmem,) * 3,
        scratch_shapes=[
            V((ROWS, CHANNELS), BF), V((CHANNELS, HID), BF), V((CHANNELS, HID), BF),
            V((HID, CHANNELS), BF), V((WIDE, CHANNELS), BF), V((TOK, WIDE), BF), V((TOK, WIDE), BF),
            V((CHANNELS, HID), BF), V((CHANNELS, HID), BF), V((HID, CHANNELS), BF),
            V((ROWS, ROWS), BF),
            chunked, chunked, chunked,
            V((NY, ROWS, WIDE), BF),
            V((ROWS, HID), BF), V((ROWS, HID), F32), V((ROWS, HID), F32), V((ROWS, HID), F32),
            V((ROWS, 2 * HID), BF), V((TOK, ROWS), BF), V((ROWS, CHANNELS), BF),
            V((CH, NY, ROWS, LANES), BF),
            halves, halves, halves, halves,
            chunked, chunked, chunked, chunked, chunked, chunked,
            V((NY, TOK, WIDE), BF),
            V((NY, 8, TOK), F32), V((NY, 8, TOK), F32),
            tokens, V((TOK, WIDE), BF), tokens, V((TOK, 1), F32), tokens, tokens, tokens,
            V((EXT, WIDE), F32), V((32, WIDE), F32),
            V((CH, 2, NX, XROWS, WIDE), BF), V((CH, NX, XROWS, WIDE), BF),
            V((CH, NX, XROWS, WIDE), BF),
            x_half, x_half, x_half, x_half,
            V((CH, XROWS, WIDE), BF), V((CH, XROWS, WIDE), BF),
            V((CH, 2 * XROWS, WIDE // 2), BF), V((CH, 2 * XROWS, WIDE // 2), BF),
            dma((7,)), dma((3,)),
            per_chunk, per_chunk, per_chunk, per_chunk,
            dma((4, CH)), per_chunk, per_chunk, per_chunk, per_chunk,
            dma((6, CH)), per_chunk, per_chunk, per_chunk, per_chunk,
            per_chunk, per_chunk, per_chunk, per_chunk,
            dma((4, CH)), per_chunk, per_chunk, per_chunk, per_chunk,
            dma((3,)), dma((1,)), dma((3,)), dma((1,)), dma((1,)), dma((1,)),
            per_chunk, per_chunk, dma((6, CH)), per_chunk, per_chunk, per_chunk, per_chunk,
            per_chunk, per_chunk,
        ],
        compiler_params=pltpu.CompilerParams(
            collective_id=0, has_side_effects=True, vmem_limit_bytes=62 * 1024 * 1024
        ),
        name="step",
    )(
        cot_out, route_ids, route_weight, conv_out, channel_norm_gain[None, :], taps,
        expert_inputs[0], w_gate[0], w_up[0], w_down[0], w_proj, value_pre, gate_pre,
    )
    return gate_grad[None], up_grad[None], down_grad[None], proj_grad, grad_value, grad_gate


def solution(mesh):
    finer = Mesh(mesh.devices.reshape(8, 4, 2, mesh.shape["tp"]), ("sp_0", "sp_1", "sp_2", "tp"))
    placed = (
        P(SP, "tp"),
        P(SP, None),
        P(SP, None),
        P(SP, None, None),
        P(SP, None, "tp"),
        P(SP, None, "tp"),
        P(SP, "tp", None),
        P("tp", None),
        P(SP, "tp"),
        P("tp"),
        P(None, "tp"),
        P(SP, "tp"),
        P(SP, "tp"),
    )
    return jax.shard_map(
        per_device,
        mesh=finer,
        in_specs=placed,
        out_specs=(
            P(SP, None, "tp"),
            P(SP, None, "tp"),
            P(SP, "tp", None),
            P(TP_SP, None),
            P(SP, "tp"),
            P(SP, "tp"),
        ),
        check_vma=False,
    )
```

time: 245 us -> 136 us (0.56)
  waiting for transfers between devices: 77 us -> 0 us
  between operations: 13.9 us -> 0.68 us
  Pallas kernels: 113 us -> 125 us
  other arithmetic: 11.4 us -> 0 us
  blocking collectives: 9.95 us -> 0 us
  starting transfers between devices: 6.28 us -> 0 us
  matrix products: 4.63 us -> 0 us
  local copies, waits for them, and re-layouts: 7.3 us -> 10.6 us
    reduce_scatter x3 -> x0, waiting for transfers between devices: 71.7 us -> none  [sum_by_axis(): subtotal = lax.psum_scatter(subtotal, axis, scatter_dimension=0, tiled=True)]
    pallas_call x1, Pallas kernels: 113 us -> 125 us  [per_device(): pl.pallas_call(step_kernel, out_shape=(jax.ShapeDtypeStruct((CHANNELS, HI...]
    psum x1 -> x0, blocking collectives: 9.95 us -> none  [per_device(): lax.psum((jnp.sum(convolution_filter, axis=1), jnp.sum(convolution_filter...]
    convert_element_type x3 -> x0, other arithmetic: 7.53 us -> none  [the longest x1 4.38 us: per_device(): (d_glu * value_pre.astype(jnp.float32) * gate_sig * (1.0 - gate_sig)).ast...]
    unnamed x15 -> x16, local copies, waits for them, and re-layouts: 4.33 us -> 10.6 us
    all_to_all x1 -> x0, waiting for transfers between devices: 5.28 us -> none  [from_everyone(): lax.all_to_all(jnp.broadcast_to(value[None], (devices, *value.shape)), ax...]
    dot_general x2 -> x0, matrix products: 4.63 us -> none  [the longest x1 2.9 us: per_device(): lax.dot_general(act_conv, mix_full, (((0,), (0,)), ((), ())), preferred_e...]
    all_to_all x1 -> x0, starting transfers between devices: 4.28 us -> none  [from_everyone(): lax.all_to_all(jnp.broadcast_to(value[None], (devices, *value.shape)), ax...]
  transfers between devices with their start and end apart: 5 -> 0, of which waited for: 4 -> 0; matrix products, arithmetic and copies ran while one was open for 4% -> 0% of each run, Pallas kernels for 0% -> 0%
where the time goes in v2:
time: 136 us
  Pallas kernels  125 us (92%)
  local copies, waits for them, and re-layouts  10.6 us (8%)
    pallas_call x1, Pallas kernels, per_device(): pl.pallas_call(step_kernel, out_shape=(jax.ShapeDtypeStruct((CHANNELS, HI...  125 us
    unnamed x16, local copies, waits for them, and re-layouts  10.6 us

profile of v2, /device:TPU:2, one launch (start us, length us, event | category | flops | bytes accessed | tf_op | source)
XLA Modules:
  0.0 135.9 jit_solution(10731872526433789180)
XLA Ops:
  0.6 1.5 %copy.19.ids = s32[256,2]{1,0:T(8,128)} copy(s32[256,2]{0,1:T(2,128)} %param.14) | data formatting | bytes 4096 | tf_op args[1]
  2.1 1.5 %copy.20.route_w = f32[256,2]{1,0:T(8,128)} copy(f32[256,2]{0,1:T(2,128)} %param.15) | data formatting | bytes 4096 | tf_op args[2]
  3.6 124.6 %step.1 = (bf16[2048,256]{1,0:T(8,128)(2,1)}, bf16[2048,256]{1,0:T(8,128)(2,1)}, bf16[256,2048]{1,0:T(8,128)(2,1)}, f32[8,2048]{1,0:T(8,128)}, bf16[256,512]{1,0:T(8,128)(2,1)}, /*index=5*/bf16[256,512]{1,0:T(8,128)(2,1)}) custom-call(bf16[256,512]{1,0:T(8,128)(2,1)} %cot.1, s32[256,2]{1,0:T(8,128)} %copy.19.ids, f32[256,2]{1,0:T(8,128)} %copy.20.route_w, ...), custom_call_target="tpu_custom_call" | custom-call | tf_op jit(solution)/shard_map/step/pallas_call | solution.py:541
  128.2 0.0 copy-start
  128.2 0.0 copy-start.3
  128.2 0.0 copy-start.2
  128.2 0.0 copy-start.1
  128.2 2.4 %copy.27 = bf16[1,2048,256]{2,1,0:T(8,128)(2,1)} copy(bf16[1,2048,256]{2,1,0:T(8,128)(2,1)} %bitcast.11) | data formatting | bytes 2097152
  130.6 2.3 %copy.28 = bf16[1,2048,256]{2,1,0:T(8,128)(2,1)} copy(bf16[1,2048,256]{2,1,0:T(8,128)(2,1)} %bitcast.10) | data formatting | bytes 2097152
  132.8 0.0 copy-done
  132.8 1.0 copy.29
  133.8 0.0 copy-done.3
  133.8 0.6 copy.30
  134.4 0.0 copy-done.2
  134.4 0.7 copy.31
  135.2 0.0 copy-done.1
  135.2 0.7 copy.32
Async XLA Ops:
  128.2 4.7 %copy-start = (bf16[256,2048]{1,0:T(8,128)(2,1)S(1)}, bf16[256,2048]{1,0:T(8,128)(2,1)}, u32[]{:S(2)}) copy-start(bf16[256,2048]{1,0:T(8,128)(2,1)} %get-tuple-element.14) | copy-start | bytes 3145732
  128.2 5.6 %copy-start.3 = (f32[8,2048]{1,0:T(8,128)S(1)}, f32[8,2048]{1,0:T(8,128)}, u32[]{:S(2)}) copy-start(f32[8,2048]{1,0:T(8,128)} %get-tuple-element.27) | copy-start | bytes 196612
  128.2 6.3 %copy-start.2 = (bf16[256,512]{1,0:T(8,128)(2,1)S(1)}, bf16[256,512]{1,0:T(8,128)(2,1)}, u32[]{:S(2)}) copy-start(bf16[256,512]{1,0:T(8,128)(2,1)} %get-tuple-element.28) | copy-start | bytes 786436
  128.2 7.0 %copy-start.1 = (bf16[256,512]{1,0:T(8,128)(2,1)S(1)}, bf16[256,512]{1,0:T(8,128)(2,1)}, u32[]{:S(2)}) copy-start(bf16[256,512]{1,0:T(8,128)(2,1)} %get-tuple-element.29) | copy-start | bytes 786436

commit v3 on v2

v3 whole, which is shorter than its diff:
```python
import functools

import jax
import jax.numpy as jnp
from jax import lax
from jax.experimental import pallas as pl
from jax.experimental.pallas import tpu as pltpu
from jax.sharding import Mesh
from jax.sharding import PartitionSpec as P

SP = ("sp_0", "sp_1", "sp_2")
TP_SP = ("tp", "sp_0", "sp_1", "sp_2")
MESH = pl.DeviceIdType.MESH

clamp_limit = 7.0
swish_alpha = 1.702
norm_epsilon = 1e-05

CH = 4
LANES = 128
NZ = 8
NG = 8
NY = 4
CAP = 12
HALVES = 2
SUB = CAP // HALVES
STEPS = HALVES * CH
BLOCK = NZ * SUB
PART = NZ * BLOCK
ROWS = HALVES * PART
HALF = PART // 2
MOST = PART - BLOCK
TOK = 256
WIDE = CH * LANES
HID = 256
TAPS = 31
FIRST_FILL = 8
DISPATCH = (
    "Z0", "Z1", "G0", "Z2", "G1", "Z3", "G2", "Y0", "Z4", "G3", "Y1", "D0", "Z5", "G4", "Y2",
    "D1", "Z6", "G5", "Y3", "D2", "Z7", "G6", "Y4", "G7", "D3", "I0",
)
BETWEEN = (
    "Y5", "D4", "P0", "Y6", "D5", "P1", "Y7", "D6", "P2", "D7", "I1",
)
RETURN = (
    "P3", "W0", "W1", "W2", "W3", "P4", "B0", "B1", "P5", "B2", "B3", "P6", "W4", "P7", "W5",
    "B4", "W6", "B5", "W7", "B6", "T0", "T1", "T2", "T3", "T4", "B7", "T5", "M0", "T6", "M1",
    "X0", "T7", "M2", "X1", "C0", "M3", "X2", "C1", "X3", "K0", "C2", "K1", "L0", "C3", "K2",
    "L1", "K3", "L2", "L3",
)
EXT = TOK + 32
CHANNELS = 2048
NX = 4
XROWS = 64
BF = jnp.bfloat16
F32 = jnp.float32


def nt(a, b):
    return lax.dot_general(a, b, (((1,), (1,)), ((), ())), preferred_element_type=F32)


def tn(a, b):
    return lax.dot_general(a, b, (((0,), (0,)), ((), ())), preferred_element_type=F32)


def nn(a, b):
    return lax.dot_general(a, b, (((1,), (0,)), ((), ())), preferred_element_type=F32)


def wait_all(ref, sem):
    pltpu.make_async_copy(ref, ref, sem).wait()


def send(src, dst, send_sem, recv_sem, device):
    pltpu.make_async_remote_copy(
        src_ref=src,
        dst_ref=dst,
        send_sem=send_sem,
        recv_sem=recv_sem,
        device_id=device,
        device_id_type=MESH,
    ).start()


def lanes(c):
    return pl.ds(c * LANES, LANES)


def rows_of(block):
    return pl.ds(pl.multiple_of(block * BLOCK, BLOCK), BLOCK)


def columns(parts, rows):
    lane = lax.broadcasted_iota(jnp.int32, (rows, LANES), 1)
    whole = jnp.zeros((rows, LANES), F32)
    for i, part in enumerate(parts):
        whole = jnp.where(lane == i, part, whole)
    return whole


def as_columns(rows8):
    return jnp.concatenate([rows8, jnp.zeros((LANES - 8, TOK), F32)], axis=0).T


def digits(at, low, high):
    rest = jnp.floor((at + 0.5) * (1.0 / low))
    top = jnp.floor((rest + 0.5) * (1.0 / high))
    return top, rest - high * top, at - low * rest


def hot_rows(source, count):
    lane = lax.broadcasted_iota(jnp.int32, (source.shape[0], count), 1).astype(F32)
    return jnp.where(lane == source, 1.0, 0.0).astype(BF)


def swap_matrix():
    at = lax.broadcasted_iota(jnp.int32, (PART, 1), 0).astype(F32)
    b, a, slot = digits(at, SUB, NZ)
    return hot_rows(a * BLOCK + b * SUB + slot, PART)


def order_matrix(half):
    at = lax.broadcasted_iota(jnp.int32, (PART, 1), 0).astype(F32)
    g, z, slot = digits(at, SUB, NZ)
    return hot_rows((z * NG + g) * CAP + half * SUB + slot, ROWS)


def step_kernel(
    cot, ids, route_w, conv, gain, taps, rows_hbm, wg_hbm, wu_hbm, wd_hbm, wp_hbm, value_hbm, gate_hbm,
    gg_hbm, gu_hbm, gd_hbm, gp_out, gv_out, gt_out,
    rows_in, wg, wu, wd, wp, value, gate, gg_out, gu_out, gd_out,
    perm, order, out_a, recv_a, out_b, cotf, act_s, f_up, f_gate, dact, up_rest, dgu, sel_t, rows_p,
    partial, r1l, r1r, accl, accr, from_l, from_r, egrad, recv_b2, out_a2, coming, mix,
    stat, nstat, xhat, act_c, fac, rstd_s, sg, vg, dac, ext, halo,
    gpb, rc, gx, x1l, x1r, xal, xar, xfl, xfr, gz, rz,
    s_in, s_out,
    s_a, r_a, s_b, r_b, s_y, r_yl, r_yr, r_fl, r_fr,
    s_rs, r_1l, r_1r, r_sl, r_sr, s_b2, r_b2, s_a2, r_a2, s_m, r_ml, r_mr, r_nl, r_nr,
    s_stat, r_stat, s_n, r_n, s_h, r_h,
    s_c, r_c, s_x, r_x1l, r_x1r, r_xl, r_xr, s_z, r_z,
):
    z = lax.axis_index("sp_0")
    x = lax.axis_index("sp_1")
    core = lax.axis_index("sp_2")
    g = x * 2 + core
    y = lax.axis_index("tp")
    right, left, across = lax.rem(y + 1, NY), lax.rem(y + 3, NY), lax.rem(y + 2, NY)
    to_right, to_left, to_across = {"tp": right}, {"tp": left}, {"tp": across}
    x_right, x_left, x_across = lax.rem(x + 1, NX), lax.rem(x + 3, NX), lax.rem(x + 2, NX)
    to_x_right, to_x_left = {"sp_1": x_right}, {"sp_1": x_left}
    to_core = {"sp_2": 1 - core}
    place = z * NG + g

    def z_peer(step):
        peer = lax.rem(z + step, NZ)
        return peer, {"sp_0": peer}

    def g_peer(step):
        peer = lax.rem(g + step, NG)
        return peer, {"sp_1": peer // 2, "sp_2": lax.rem(peer, 2)}

    def in_line(step):
        other = lax.rem(place + step, NZ * NG)
        return {"sp_0": other // NG, "sp_1": lax.rem(other // 2, NX), "sp_2": lax.rem(other, 2)}

    to_before = in_line(NZ * NG - 1)
    barrier = pltpu.get_barrier_semaphore()
    greeted = [z_peer(step)[1] for step in range(1, NZ)] + [g_peer(step)[1] for step in range(1, NG)]
    greeted += [to_right, to_left, to_across, to_before, in_line(1)]
    for device in greeted:
        pl.semaphore_signal(barrier, inc=1, device_id=device, device_id_type=MESH)

    fetches = [
        pltpu.make_async_copy(src, dst, s_in.at[i])
        for i, (src, dst) in enumerate(
            ((rows_hbm, rows_in), (wg_hbm, wg), (wu_hbm, wu), (wd_hbm, wd),
             (gate_hbm, gate), (value_hbm, value), (wp_hbm, wp))
        )
    ]
    for fetch in fetches:
        fetch.start()

    t_sub = lax.broadcasted_iota(jnp.int32, (TOK, TOK), 0)
    t_lane = lax.broadcasted_iota(jnp.int32, (TOK, TOK), 1)
    before, after = t_sub < t_lane, t_lane < t_sub
    row = [ids[k : k + 1, :].astype(F32) for k in (0, 1)]
    w_r = [route_w[k : k + 1, :] for k in (0, 1)]
    turned = as_columns(jnp.concatenate(row + [jnp.zeros((6, TOK), F32)], axis=0))
    col = [turned[:, k : k + 1] for k in (0, 1)]

    def row_of(slot, expert):
        return slot + SUB * expert + jnp.where(slot >= SUB, 1.0 * (PART - SUB), 0.0)

    slot_r = lax.broadcasted_iota(jnp.int32, (ROWS, TOK), 0).astype(F32)
    chosen, weight = None, None
    for k in (0, 1):
        same = ((col[0] == row[k]) | (col[1] == row[k])) & before
        dest = row_of(jnp.sum(jnp.where(same, 1.0, 0.0), axis=0, keepdims=True), row[k])
        hot = slot_r == dest
        one, scale = jnp.where(hot, 1.0, 0.0), jnp.where(hot, w_r[k], 0.0)
        chosen = one if chosen is None else chosen + one
        weight = scale if weight is None else weight + scale
    chosen = chosen.astype(BF)
    weight = jnp.sum(weight, axis=1, keepdims=True)

    for i in range(STEPS):
        c, part = i % CH, slice(i // CH * PART, i // CH * PART + PART)
        out_a[i] = (weight[part] * nn(chosen[part], cot[:, lanes(c)])).astype(BF)
        if i == 0:
            pl.semaphore_wait(barrier, len(greeted))
        for step in (4, 3, 5, 2, 6, 1, 7):
            peer, device = z_peer(step)
            send(out_a.at[i, rows_of(peer)], recv_a.at[i, rows_of(z)], s_a.at[i], r_a.at[i], device)
        recv_a[i, rows_of(z), :] = out_a[i, rows_of(z), :]

    wide = conv[...].astype(F32)
    sums = [jnp.sum(v, axis=1, keepdims=True) for v in (wide, wide * wide)]
    stat[y] = columns(sums, TOK).T[0:8, :]
    for i, device in enumerate((to_right, to_left, to_across)):
        send(stat.at[y], stat.at[y], s_stat.at[i], r_stat.at[0], device)

    perm[...] = swap_matrix()

    def unpack_slots():
        slot_c = lax.broadcasted_iota(jnp.int32, (TOK, ROWS), 1).astype(F32)
        back = None
        for k in (0, 1):
            same = ((row[0] == col[k]) | (row[1] == col[k])) & after
            dest = row_of(jnp.sum(jnp.where(same, 1.0, 0.0), axis=1, keepdims=True), col[k])
            one = jnp.where(slot_c == dest, 1.0, 0.0)
            back = one if back is None else back + one
        sel_t[...] = back.astype(BF)

    def forward_rows(half, j):
        if j == 0:
            if half == 0:
                fetches[0].wait()
            order[...] = order_matrix(half)
        cols = pl.ds(j * 512, 512)
        rows_p[pl.ds(half * PART, PART), cols] = nn(order[...], rows_in[:, cols]).astype(BF)

    def forward_sums(j):
        total, w = ((f_gate, wg), (f_up, wu), (dact, wg), (up_rest, wu))[j]
        if j < 2:
            fetches[j + 1].wait()
        half = pl.ds(j // 2 * (CHANNELS // 2), CHANNELS // 2)
        total[...] = nn(rows_p[:, half], w[half, :])

    def forward_part(j):
        part = pl.ds(j * 256, 256)
        gate_lin = f_gate[part, :] + dact[part, :]
        up_lin = f_up[part, :] + up_rest[part, :]
        gate_c = jnp.minimum(gate_lin, clamp_limit)
        up_c = jnp.clip(up_lin, -clamp_limit, clamp_limit)
        sig = jax.nn.sigmoid(swish_alpha * gate_c)
        act_s[part, :] = ((up_c + 1.0) * gate_c * sig).astype(BF)
        up_open = (up_lin > -clamp_limit) & (up_lin < clamp_limit)
        f_up[part, :] = jnp.where(up_open, gate_c * sig, 0.0)
        slope = (up_c + 1.0) * (sig + swish_alpha * gate_c * sig * (1.0 - sig))
        f_gate[part, :] = jnp.where(gate_lin < clamp_limit, slope, 0.0)

    def norm_terms():
        wait_all(stat.at[pl.ds(0, NY - 1)], r_stat.at[0])
        total = as_columns(stat[0] + stat[1] + stat[2] + stat[3])
        mean = total[:, 0:1] / CHANNELS
        var = total[:, 1:2] / CHANNELS - mean * mean
        rstd = lax.rsqrt(var + norm_epsilon)
        rstd_s[...] = rstd
        normalized = (conv[...].astype(F32) - mean) * rstd
        xhat[...] = normalized
        normed = normalized * gain[...]
        s = jax.nn.sigmoid(normed)
        act_c[...] = (normed * s).astype(BF)
        fac[...] = s * (1.0 + normed * (1.0 - s)) * gain[...]

    def glu_terms():
        fetches[4].wait()
        fetches[5].wait()
        gate_sig = jax.nn.sigmoid(gate[...].astype(F32))
        sg[...] = gate_sig
        vg[...] = value[...].astype(F32) * gate_sig * (1.0 - gate_sig)
        fetches[6].wait()

    fill = [functools.partial(forward_rows, half, j) for half in range(HALVES) for j in range(4)]
    fill += [functools.partial(forward_sums, j) for j in range(4)]
    fill += [functools.partial(forward_part, j) for j in range(3)]
    fill += [fetches[3].wait, norm_terms, unpack_slots, glu_terms]
    for _ in range(FIRST_FILL):
        fill.pop(0)()

    def rows_at(i):
        return pl.ds(i // CH * PART, PART)

    def half_at(i, which):
        return pl.ds(i // CH * PART + which * HALF, HALF)

    low, high = pl.ds(0, HALF), pl.ds(HALF, HALF)

    def from_z(i):
        wait_all(recv_a.at[i, pl.ds(0, MOST)], r_a.at[i])
        out_b[i] = nn(perm[...], recv_a[i]).astype(BF)
        mine = pl.ds(pl.multiple_of(i // CH * PART + g * BLOCK, BLOCK), BLOCK)
        for step in (4, 2, 6, 3, 5, 1, 7):
            peer, device = g_peer(step)
            send(
                out_b.at[i, rows_of(peer)], cotf.at[y, mine, lanes(i % CH)],
                s_b.at[i], r_b.at[i], device,
            )
        cotf[y, mine, lanes(i % CH)] = out_b[i, rows_of(g), :]

    def from_g(i):
        wait_all(out_b.at[i, pl.ds(0, MOST)], r_b.at[i])
        mine = cotf.at[y, rows_at(i), lanes(i % CH)]
        send(mine, mine, s_y.at[0, i], r_yl.at[i], to_right)
        send(mine, mine, s_y.at[1, i], r_yr.at[i], to_left)

    def from_y(i):
        wait_all(out_b.at[i], r_yl.at[i])
        passed = cotf.at[left, half_at(i, 0), lanes(i % CH)]
        send(passed, passed, s_y.at[2, i], r_fl.at[i], to_right)
        wait_all(out_b.at[i], r_yr.at[i])
        passed = cotf.at[right, half_at(i, 1), lanes(i % CH)]
        send(passed, passed, s_y.at[3, i], r_fr.at[i], to_left)

    def gathered(i):
        c, part = i % CH, rows_at(i)
        wait_all(out_b.at[i, low], r_fl.at[i])
        wait_all(out_b.at[i, low], r_fr.at[i])
        arrived = jnp.concatenate([cotf[q, part, lanes(c)] for q in range(NY)], axis=1)
        down = jnp.concatenate(
            [wd[:, pl.ds(q * WIDE + c * LANES, LANES)] for q in range(NY)], axis=1
        )
        term = nt(arrived, down)
        dact[part, :] = term if c == 0 else dact[part, :] + term

    def input_grads(half):
        part = pl.ds(half * PART, PART)
        dgu[part, 0:HID] = (dact[part, :] * f_gate[part, :]).astype(BF)
        dgu[part, HID : 2 * HID] = (dact[part, :] * f_up[part, :]).astype(BF)
        for c in range(CH):
            i = half * CH + c
            weights = jnp.concatenate(
                [
                    jnp.concatenate(
                        [w[pl.ds(q * WIDE + c * LANES, LANES), :] for w in (wg, wu)], axis=1
                    )
                    for q in range(NY)
                ],
                axis=0,
            )
            product = nt(dgu[part, :], weights).astype(BF)
            for q in range(NY):
                partial[i, q] = product[:, q * LANES : (q + 1) * LANES]
            send(partial.at[i, across, low], r1l.at[i], s_rs.at[0, i], r_1l.at[i], to_right)
            send(partial.at[i, across, high], r1r.at[i], s_rs.at[1, i], r_1r.at[i], to_left)
            send(partial.at[i, right, high], from_l.at[i, high], s_rs.at[2, i], r_sl.at[i], to_right)
            send(partial.at[i, left, low], from_r.at[i, low], s_rs.at[3, i], r_sr.at[i], to_left)

    def partial_sums(i):
        wait_all(r1l.at[i], r_1l.at[i])
        accr[i] = (partial[i, right, low, :].astype(F32) + r1l[i].astype(F32)).astype(BF)
        send(accr.at[i], from_l.at[i, low], s_rs.at[4, i], r_sl.at[i], to_right)
        wait_all(r1r.at[i], r_1r.at[i])
        accl[i] = (partial[i, left, high, :].astype(F32) + r1r[i].astype(F32)).astype(BF)
        send(accl.at[i], from_r.at[i, high], s_rs.at[5, i], r_sr.at[i], to_left)

    def whole_sums(i):
        wait_all(from_l.at[i], r_sl.at[i])
        wait_all(from_r.at[i], r_sr.at[i])
        total = partial[i, y].astype(F32) + from_l[i].astype(F32) + from_r[i].astype(F32)
        egrad[i] = total.astype(BF)
        for step in (4, 2, 6, 3, 5, 1, 7):
            peer, device = g_peer(step)
            send(
                egrad.at[i, rows_of(peer)], recv_b2.at[i, rows_of(g)],
                s_b2.at[i], r_b2.at[i], device,
            )
        recv_b2[i, rows_of(g), :] = egrad[i, rows_of(g), :]

    def back_to_z(i):
        wait_all(recv_b2.at[i, pl.ds(0, MOST)], r_b2.at[i])
        out_a2[i] = nn(perm[...], recv_b2[i]).astype(BF)
        for step in (4, 3, 5, 2, 6, 1, 7):
            peer, device = z_peer(step)
            send(
                out_a2.at[i, rows_of(peer)], coming.at[i, rows_of(z)],
                s_a2.at[i], r_a2.at[i], device,
            )
        coming[i, rows_of(z), :] = out_a2[i, rows_of(z), :]

    def at_tokens(i):
        wait_all(coming.at[i, pl.ds(0, MOST)], r_a2.at[i])
        c = i - (STEPS - CH)
        if c >= 0:
            summed = nn(sel_t[:, 0:PART], coming[c]) + nn(sel_t[:, PART:ROWS], coming[i])
            mix[y, :, lanes(c)] = (cot[:, lanes(c)].astype(F32) + summed).astype(BF)
            mine = mix.at[y, :, lanes(c)]
            send(mine, mine, s_m.at[0, c], r_ml.at[c], to_right)
            send(mine, mine, s_m.at[1, c], r_mr.at[c], to_left)

    def mix_passed(c):
        size = coming.at[c, pl.ds(0, TOK)]
        wait_all(size, r_ml.at[c])
        passed = mix.at[left, pl.ds(0, TOK // 2), lanes(c)]
        send(passed, passed, s_m.at[2, c], r_nl.at[c], to_right)
        wait_all(size, r_mr.at[c])
        passed = mix.at[right, pl.ds(TOK // 2, TOK // 2), lanes(c)]
        send(passed, passed, s_m.at[3, c], r_nr.at[c], to_left)

    def mix_whole(c):
        size = coming.at[c, pl.ds(0, TOK // 2)]
        wait_all(size, r_nl.at[c])
        wait_all(size, r_nr.at[c])
        arrived = jnp.concatenate([mix[q, :, lanes(c)] for q in range(NY)], axis=1)
        proj = jnp.concatenate(
            [wp[:, pl.ds(q * WIDE + c * LANES, LANES)] for q in range(NY)], axis=1
        )
        term = nt(arrived, proj)
        dac[...] = term if c == 0 else dac[...] + term
        if c == CH - 1:
            norm_grad_sums()
        product = tn(act_c[...], arrived)
        for core_at in range(2):
            for x_at in range(NX):
                gpb[c, core_at, x_at] = jnp.concatenate(
                    [
                        product[(z_at * NG + x_at * 2 + core_at) * 8 :][:8]
                        for z_at in range(NZ)
                    ],
                    axis=0,
                ).astype(BF)
        send(gpb.at[c, 1 - core], rc.at[c], s_c.at[c], r_c.at[c], to_core)

    def core_sums(c):
        wait_all(rc.at[c], r_c.at[c])
        gx[c] = (gpb[c, core].astype(F32) + rc[c].astype(F32)).astype(BF)
        top, bottom = pl.ds(0, XROWS // 2), pl.ds(XROWS // 2, XROWS // 2)
        send(gx.at[c, x_across, top], x1l.at[c], s_x.at[0, c], r_x1l.at[c], to_x_right)
        send(gx.at[c, x_across, bottom], x1r.at[c], s_x.at[1, c], r_x1r.at[c], to_x_left)
        send(gx.at[c, x_right, bottom], xfl.at[c, bottom], s_x.at[2, c], r_xl.at[c], to_x_right)
        send(gx.at[c, x_left, top], xfr.at[c, top], s_x.at[3, c], r_xr.at[c], to_x_left)

    def x_partial(c):
        top, bottom = pl.ds(0, XROWS // 2), pl.ds(XROWS // 2, XROWS // 2)
        wait_all(x1l.at[c], r_x1l.at[c])
        xar[c] = (gx[c, x_right, top, :].astype(F32) + x1l[c].astype(F32)).astype(BF)
        send(xar.at[c], xfl.at[c, top], s_x.at[4, c], r_xl.at[c], to_x_right)
        wait_all(x1r.at[c], r_x1r.at[c])
        xal[c] = (gx[c, x_left, bottom, :].astype(F32) + x1r[c].astype(F32)).astype(BF)
        send(xal.at[c], xfr.at[c, bottom], s_x.at[5, c], r_xr.at[c], to_x_left)
        if c == CH - 2:
            conv_grad()

    def x_whole(c):
        wait_all(xfl.at[c], r_xl.at[c])
        wait_all(xfr.at[c], r_xr.at[c])
        total = gx[c, x].astype(F32) + xfl[c].astype(F32) + xfr[c].astype(F32)
        gz[c] = jnp.concatenate(
            [
                total[z_at * 8 : z_at * 8 + 8, half * 256 : half * 256 + 256]
                for z_at in range(NZ)
                for half in (0, 1)
            ],
            axis=0,
        ).astype(BF)
        for step in (4, 3, 5, 2, 6, 1, 7):
            peer, device = z_peer(step)
            send(
                gz.at[c, pl.ds(pl.multiple_of(peer * 16, 16), 16)],
                rz.at[c, pl.ds(pl.multiple_of(z * 16, 16), 16)],
                s_z.at[c], r_z.at[c], device,
            )
        own = pl.ds(pl.multiple_of(z * 16, 16), 16)
        rz[c, own, :] = gz[c, own, :]
        if c == CH - 2:
            conv_first()
        if c == CH - 1:
            conv_rest()

    def weight_grads(j):
        if j < 4:
            gd_out[:, pl.ds(j * WIDE, WIDE)] = tn(act_s[...], cotf[j]).astype(BF)
        else:
            part = pl.ds((j - 4) * 256, 256)
            both = tn(rows_p[:, part], dgu[...]).astype(BF)
            gg_out[part, :] = both[:, 0:HID]
            gu_out[part, :] = both[:, HID : 2 * HID]

    stores = [
        pltpu.make_async_copy(src, dst, s_out.at[i])
        for i, (src, dst) in enumerate(((gg_out, gg_hbm), (gu_out, gu_hbm), (gd_out, gd_hbm)))
    ]

    def norm_grad_sums():
        grad = dac[...] * fac[...]
        dac[...] = grad
        sums = [jnp.sum(v, axis=1, keepdims=True) for v in (grad, grad * xhat[...])]
        nstat[y] = columns(sums, TOK).T[0:8, :]
        for i, device in enumerate((to_right, to_left, to_across)):
            send(nstat.at[y], nstat.at[y], s_n.at[i], r_n.at[0], device)

    def conv_grad():
        wait_all(nstat.at[pl.ds(0, NY - 1)], r_n.at[0])
        total = as_columns(nstat[0] + nstat[1] + nstat[2] + nstat[3]) / CHANNELS
        ext[0:TOK, :] = rstd_s[...] * (dac[...] - total[:, 0:1] - xhat[...] * total[:, 1:2])
        send(ext.at[pl.ds(0, 32)], halo, s_h.at[0], r_h.at[0], to_before)

    def conv_rows(begin):
        part = pl.ds(begin, TOK // 2)

        def column(j, carry):
            cols = pl.ds(pl.multiple_of(j * LANES, LANES), LANES)
            total = jnp.zeros((TOK // 2, LANES), F32)
            for k in range(TAPS):
                total = total + taps[k : k + 1, cols] * ext[pl.ds(begin + TAPS - 1 - k, TOK // 2), cols]
            gv_out[part, cols] = (total * sg[part, cols]).astype(BF)
            gt_out[part, cols] = (total * vg[part, cols]).astype(BF)
            return carry

        lax.fori_loop(0, CH, column, 0)

    def conv_first():
        conv_rows(0)

    def conv_rest():
        wait_all(halo, r_h.at[0])
        keep = jnp.where(place == NZ * NG - 1, 0.0, 1.0)
        ext[TOK:EXT, :] = halo[...] * keep
        conv_rows(TOK // 2)

    stages = dict(
        Z=from_z, G=from_g, Y=from_y, D=gathered, I=input_grads, P=partial_sums, W=whole_sums,
        B=back_to_z, T=at_tokens, M=mix_passed, X=mix_whole, C=core_sums, K=x_partial, L=x_whole,
    )

    def run(order, beside):
        for name in order:
            stages[name[0]](int(name[1]))
            if beside:
                beside.pop(0)()

    run(DISPATCH, fill)
    run(BETWEEN, fill)
    grads = [functools.partial(weight_grads, j) for j in range(4)] + [stores[2].start]
    grads += [functools.partial(weight_grads, j) for j in range(4, 12)]
    grads += [stores[0].start, stores[1].start]
    run(RETURN, grads)

    for c in range(CH):
        wait_all(rz.at[c, pl.ds(0, 112)], r_z.at[c])
        total = rz[c, 0:16, :].astype(F32)
        for z_at in range(1, NZ):
            total = total + rz[c, z_at * 16 : z_at * 16 + 16, :].astype(F32)
        for q in range(NY):
            row_at, lane_at = (q // 2) * 8, (q % 2) * LANES
            gp_out[:, pl.ds(q * WIDE + c * LANES, LANES)] = total[
                row_at : row_at + 8, lane_at : lane_at + LANES
            ]

    for i in range(STEPS):
        full, most, half = out_b.at[i], out_b.at[i, pl.ds(0, MOST)], out_b.at[i, low]
        for sem in (s_a, s_b, s_b2, s_a2):
            wait_all(most, sem.at[i])
        for j, size in enumerate((full, full, half, half)):
            wait_all(size, s_y.at[j, i])
        for j in range(6):
            wait_all(half, s_rs.at[j, i])
    for c in range(CH):
        for i in range(4):
            wait_all(out_b.at[c, pl.ds(0, TOK if i < 2 else TOK // 2)], s_m.at[i, c])
        wait_all(rc.at[c], s_c.at[c])
        for i in range(6):
            wait_all(x1l.at[c], s_x.at[i, c])
        wait_all(rz.at[c, pl.ds(0, 112)], s_z.at[c])
    for i in range(3):
        wait_all(stat.at[0], s_stat.at[i])
        wait_all(nstat.at[0], s_n.at[i])
        stores[i].wait()
    wait_all(halo, s_h.at[0])


def hand_on_kernel(*refs):
    count = (len(refs) - 2) // 3
    sources, results, held = refs[:count], refs[count : 2 * count], refs[2 * count : 3 * count]
    s_in, s_out = refs[3 * count :]
    reads = [pltpu.make_async_copy(a, b, s_in.at[i]) for i, (a, b) in enumerate(zip(sources, held))]
    writes = [pltpu.make_async_copy(a, b, s_out.at[i]) for i, (a, b) in enumerate(zip(held, results))]
    for read in reads:
        read.start()
    for read, write in zip(reads, writes):
        read.wait()
        write.start()
    for write in writes:
        write.wait()


def handed_on(*arrays):
    anywhere = pl.BlockSpec(memory_space=pl.ANY)
    return pl.pallas_call(
        hand_on_kernel,
        out_shape=tuple(jax.ShapeDtypeStruct(a.shape, a.dtype) for a in arrays),
        in_specs=[anywhere] * len(arrays),
        out_specs=(anywhere,) * len(arrays),
        scratch_shapes=[pltpu.VMEM(a.shape, a.dtype) for a in arrays]
        + [pltpu.SemaphoreType.DMA((len(arrays),))] * 2,
        name="handed_on",
    )(*arrays)


def per_device(
    cot_out,
    route_ids,
    route_weight,
    expert_inputs,
    w_gate,
    w_up,
    w_down,
    w_proj,
    conv_out,
    channel_norm_gain,
    taps,
    value_pre,
    gate_pre,
):
    vmem = pl.BlockSpec(memory_space=pltpu.VMEM)
    anywhere = pl.BlockSpec(memory_space=pl.ANY)
    dma, V = pltpu.SemaphoreType.DMA, pltpu.VMEM
    chunked = V((STEPS, PART, LANES), BF)
    halves = V((STEPS, HALF, LANES), BF)
    tokens = V((TOK, WIDE), F32)
    x_half = V((CH, XROWS // 2, WIDE), BF)
    per_chunk, per_step = dma((CH,)), dma((STEPS,))
    gate_grad, up_grad, down_grad, proj_grad, grad_value, grad_gate = pl.pallas_call(
        step_kernel,
        out_shape=(
            jax.ShapeDtypeStruct((CHANNELS, HID), BF),
            jax.ShapeDtypeStruct((CHANNELS, HID), BF),
            jax.ShapeDtypeStruct((HID, CHANNELS), BF),
            jax.ShapeDtypeStruct((8, CHANNELS), F32),
            jax.ShapeDtypeStruct((TOK, WIDE), BF),
            jax.ShapeDtypeStruct((TOK, WIDE), BF),
        ),
        in_specs=[vmem] * 6 + [anywhere] * 7,
        out_specs=(anywhere,) * 3 + (vmem,) * 3,
        scratch_shapes=[
            V((ROWS, CHANNELS), BF), V((CHANNELS, HID), BF), V((CHANNELS, HID), BF),
            V((HID, CHANNELS), BF), V((WIDE, CHANNELS), BF), V((TOK, WIDE), BF), V((TOK, WIDE), BF),
            V((CHANNELS, HID), BF), V((CHANNELS, HID), BF), V((HID, CHANNELS), BF),
            V((PART, PART), BF), V((PART, ROWS), BF),
            chunked, chunked, chunked,
            V((NY, ROWS, WIDE), BF),
            V((ROWS, HID), BF), V((ROWS, HID), F32), V((ROWS, HID), F32), V((ROWS, HID), F32),
            V((ROWS, HID), F32),
            V((ROWS, 2 * HID), BF), V((TOK, ROWS), BF), V((ROWS, CHANNELS), BF),
            V((STEPS, NY, PART, LANES), BF),
            halves, halves, halves, halves,
            chunked, chunked, chunked, chunked, chunked, chunked,
            V((NY, TOK, WIDE), BF),
            V((NY, 8, TOK), F32), V((NY, 8, TOK), F32),
            tokens, V((TOK, WIDE), BF), tokens, V((TOK, 1), F32), tokens, tokens, tokens,
            V((EXT, WIDE), F32), V((32, WIDE), F32),
            V((CH, 2, NX, XROWS, WIDE), BF), V((CH, NX, XROWS, WIDE), BF),
            V((CH, NX, XROWS, WIDE), BF),
            x_half, x_half, x_half, x_half,
            V((CH, XROWS, WIDE), BF), V((CH, XROWS, WIDE), BF),
            V((CH, 2 * XROWS, WIDE // 2), BF), V((CH, 2 * XROWS, WIDE // 2), BF),
            dma((7,)), dma((3,)),
            per_step, per_step, per_step, per_step,
            dma((4, STEPS)), per_step, per_step, per_step, per_step,
            dma((6, STEPS)), per_step, per_step, per_step, per_step,
            per_step, per_step, per_step, per_step,
            dma((4, CH)), per_chunk, per_chunk, per_chunk, per_chunk,
            dma((3,)), dma((1,)), dma((3,)), dma((1,)), dma((1,)), dma((1,)),
            per_chunk, per_chunk, dma((6, CH)), per_chunk, per_chunk, per_chunk, per_chunk,
            per_chunk, per_chunk,
        ],
        compiler_params=pltpu.CompilerParams(
            collective_id=0, has_side_effects=True, vmem_limit_bytes=62 * 1024 * 1024
        ),
        name="step",
    )(
        cot_out, route_ids.T, route_weight.T, conv_out, channel_norm_gain[None, :], taps,
        expert_inputs[0], w_gate[0], w_up[0], w_down[0], w_proj, value_pre, gate_pre,
    )
    gate_grad, up_grad, down_grad, proj_grad, grad_value, grad_gate = handed_on(
        gate_grad, up_grad, down_grad, proj_grad, grad_value, grad_gate
    )
    return gate_grad[None], up_grad[None], down_grad[None], proj_grad, grad_value, grad_gate


def solution(mesh):
    finer = Mesh(mesh.devices.reshape(8, 4, 2, mesh.shape["tp"]), ("sp_0", "sp_1", "sp_2", "tp"))
    placed = (
        P(SP, "tp"),
        P(SP, None),
        P(SP, None),
        P(SP, None, None),
        P(SP, None, "tp"),
        P(SP, None, "tp"),
        P(SP, "tp", None),
        P("tp", None),
        P(SP, "tp"),
        P("tp"),
        P(None, "tp"),
        P(SP, "tp"),
        P(SP, "tp"),
    )
    return jax.shard_map(
        per_device,
        mesh=finer,
        in_specs=placed,
        out_specs=(
            P(SP, None, "tp"),
            P(SP, None, "tp"),
            P(SP, "tp", None),
            P(TP_SP, None),
            P(SP, "tp"),
            P(SP, "tp"),
        ),
        check_vma=False,
    )
```

time: 136 us -> 125 us (0.919)
  local copies, waits for them, and re-layouts: 10.6 us -> 0 us
    unnamed x16 -> x0, local copies, waits for them, and re-layouts: 10.6 us -> none
    pallas_call x1, Pallas kernels: 125 us -> 121 us  [per_device(): pl.pallas_call(step_kernel, out_shape=(jax.ShapeDtypeStruct((CHANNELS, HI...]
    pallas_call x0 -> x1, Pallas kernels: none -> 3.18 us  [handed_on(): pl.pallas_call(hand_on_kernel, out_shape=tuple((jax.ShapeDtypeStruct(a.sh...]
where the time goes in v3:
time: 125 us
  Pallas kernels  124 us (99%)
    pallas_call x1, Pallas kernels, per_device(): pl.pallas_call(step_kernel, out_shape=(jax.ShapeDtypeStruct((CHANNELS, HI...  121 us
    pallas_call x1, Pallas kernels, handed_on(): pl.pallas_call(hand_on_kernel, out_shape=tuple((jax.ShapeDtypeStruct(a.sh...  3.18 us

profile of v3, /device:TPU:2, one launch (start us, length us, event | category | flops | bytes accessed | tf_op | source)
XLA Modules:
  0.0 125.0 jit_solution(11114622632531083445)
XLA Ops:
  0.6 121.0 %step.1 = (bf16[2048,256]{1,0:T(8,128)(2,1)}, bf16[2048,256]{1,0:T(8,128)(2,1)}, bf16[256,2048]{1,0:T(8,128)(2,1)}, f32[8,2048]{1,0:T(8,128)}, bf16[256,512]{1,0:T(8,128)(2,1)}, /*index=5*/bf16[256,512]{1,0:T(8,128)(2,1)}) custom-call(bf16[256,512]{1,0:T(8,128)(2,1)} %cot.1, s32[2,256]{1,0:T(2,128)} %bitcast.14, f32[2,256]{1,0:T(2,128)} %bitcast.15, ...), custom_call_target="tpu_custom_call" | custom-call | tf_op jit(solution)/shard_map/step/pallas_call | solution.py:634
  121.7 3.2 %handed_on.1 = (bf16[2048,256]{1,0:T(8,128)(2,1)}, bf16[2048,256]{1,0:T(8,128)(2,1)}, bf16[256,2048]{1,0:T(8,128)(2,1)}, f32[8,2048]{1,0:T(8,128)}, bf16[256,512]{1,0:T(8,128)(2,1)}, /*index=5*/bf16[256,512]{1,0:T(8,128)(2,1)}) custom-call(bf16[2048,256]{1,0:T(8,128)(2,1)} %get-tuple-element.18.refs_0_, bf16[2048,256]{1,0:T(8,128)(2,1)} %get-tuple-element.19.refs_1_, ...), custom_call_target="tpu_custom_call" | custom-call | tf_op jit(solution)/shard_map/handed_on/pallas_call | solution.py:600

commit v4 on v3

--- a/solution.py
+++ b/solution.py
@@ -35,6 +35,7 @@
 HID = 256
 TAPS = 31
 FIRST_FILL = 8
+AHEAD = 2
 DISPATCH = (
     "Z0", "Z1", "G0", "Z2", "G1", "Z3", "G2", "Y0", "Z4", "G3", "Y1", "D0", "Z5", "G4", "Y2",
     "D1", "Z6", "G5", "Y3", "D2", "Z7", "G6", "Y4", "G7", "D3", "I0",
@@ -43,10 +44,10 @@
     "Y5", "D4", "P0", "Y6", "D5", "P1", "Y7", "D6", "P2", "D7", "I1",
 )
 RETURN = (
-    "P3", "W0", "W1", "W2", "W3", "P4", "B0", "B1", "P5", "B2", "B3", "P6", "W4", "P7", "W5",
-    "B4", "W6", "B5", "W7", "B6", "T0", "T1", "T2", "T3", "T4", "B7", "T5", "M0", "T6", "M1",
-    "X0", "T7", "M2", "X1", "C0", "M3", "X2", "C1", "X3", "K0", "C2", "K1", "L0", "C3", "K2",
-    "L1", "K3", "L2", "L3",
+    "P3", "W0", "W1", "P4", "W2", "W3", "B0", "B1", "P5", "B2", "W4", "B3", "P6", "W5",
+    "T0", "B4", "T1", "P7", "W6", "T2", "B5", "T3", "W7", "B6", "T4", "B7", "T5", "M0",
+    "T6", "M1", "X0", "T7", "M2", "X1", "C0", "M3", "X2", "C1", "X3", "K0", "C2", "K1",
+    "L0", "C3", "K2", "L1", "K3", "L2", "L3",
 )
 EXT = TOK + 32
 CHANNELS = 2048
@@ -271,7 +272,7 @@
         xhat[...] = normalized
         normed = normalized * gain[...]
         s = jax.nn.sigmoid(normed)
-        act_c[...] = (normed * s).astype(BF)
+        act_c[...] = (normed * s).T.astype(BF)
         fac[...] = s * (1.0 + normed * (1.0 - s)) * gain[...]
 
     def glu_terms():
@@ -333,6 +334,12 @@
         )
         term = nt(arrived, down)
         dact[part, :] = term if c == 0 else dact[part, :] + term
+
+    def first_partials(i):
+        send(partial.at[i, across, low], r1l.at[i], s_rs.at[0, i], r_1l.at[i], to_right)
+        send(partial.at[i, across, high], r1r.at[i], s_rs.at[1, i], r_1r.at[i], to_left)
+        send(partial.at[i, right, high], from_l.at[i, high], s_rs.at[2, i], r_sl.at[i], to_right)
+        send(partial.at[i, left, low], from_r.at[i, low], s_rs.at[3, i], r_sr.at[i], to_left)
 
     def input_grads(half):
         part = pl.ds(half * PART, PART)
@@ -352,10 +359,8 @@
             product = nt(dgu[part, :], weights).astype(BF)
             for q in range(NY):
                 partial[i, q] = product[:, q * LANES : (q + 1) * LANES]
-            send(partial.at[i, across, low], r1l.at[i], s_rs.at[0, i], r_1l.at[i], to_right)
-            send(partial.at[i, across, high], r1r.at[i], s_rs.at[1, i], r_1r.at[i], to_left)
-            send(partial.at[i, right, high], from_l.at[i, high], s_rs.at[2, i], r_sl.at[i], to_right)
-            send(partial.at[i, left, low], from_r.at[i, low], s_rs.at[3, i], r_sr.at[i], to_left)
+            if c < AHEAD:
+                first_partials(i)
 
     def partial_sums(i):
         wait_all(r1l.at[i], r_1l.at[i])
@@ -364,6 +369,8 @@
         wait_all(r1r.at[i], r_1r.at[i])
         accl[i] = (partial[i, left, high, :].astype(F32) + r1r[i].astype(F32)).astype(BF)
         send(accl.at[i], from_r.at[i, high], s_rs.at[5, i], r_sr.at[i], to_left)
+        if i % CH + AHEAD < CH:
+            first_partials(i + AHEAD)
 
     def whole_sums(i):
         wait_all(from_l.at[i], r_sl.at[i])
@@ -392,9 +399,12 @@
     def at_tokens(i):
         wait_all(coming.at[i, pl.ds(0, MOST)], r_a2.at[i])
         c = i - (STEPS - CH)
-        if c >= 0:
-            summed = nn(sel_t[:, 0:PART], coming[c]) + nn(sel_t[:, PART:ROWS], coming[i])
-            mix[y, :, lanes(c)] = (cot[:, lanes(c)].astype(F32) + summed).astype(BF)
+        if c < 0:
+            first = nn(sel_t[:, 0:PART], coming[i])
+            ext[0:TOK, lanes(i)] = cot[:, lanes(i)].astype(F32) + first
+        else:
+            summed = ext[0:TOK, lanes(c)] + nn(sel_t[:, PART:ROWS], coming[i])
+            mix[y, :, lanes(c)] = summed.astype(BF)
             mine = mix.at[y, :, lanes(c)]
             send(mine, mine, s_m.at[0, c], r_ml.at[c], to_right)
             send(mine, mine, s_m.at[1, c], r_mr.at[c], to_left)
@@ -420,7 +430,7 @@
         dac[...] = term if c == 0 else dac[...] + term
         if c == CH - 1:
             norm_grad_sums()
-        product = tn(act_c[...], arrived)
+        product = nn(act_c[...], arrived)
         for core_at in range(2):
             for x_at in range(NX):
                 gpb[c, core_at, x_at] = jnp.concatenate(
@@ -658,7 +668,7 @@
             chunked, chunked, chunked, chunked, chunked, chunked,
             V((NY, TOK, WIDE), BF),
             V((NY, 8, TOK), F32), V((NY, 8, TOK), F32),
-            tokens, V((TOK, WIDE), BF), tokens, V((TOK, 1), F32), tokens, tokens, tokens,
+            tokens, V((WIDE, TOK), BF), tokens, V((TOK, 1), F32), tokens, tokens, tokens,
             V((EXT, WIDE), F32), V((32, WIDE), F32),
             V((CH, 2, NX, XROWS, WIDE), BF), V((CH, NX, XROWS, WIDE), BF),
             V((CH, NX, XROWS, WIDE), BF),

time: 125 us -> 120 us (0.960)
  Pallas kernels: 124 us -> 119 us
    pallas_call x1, Pallas kernels: 121 us -> 116 us  [per_device(): pl.pallas_call(step_kernel, out_shape=(jax.ShapeDtypeStruct((CHANNELS, HI...]
where the time goes in v4:
time: 120 us
  Pallas kernels  119 us (99%)
    pallas_call x1, Pallas kernels, per_device(): pl.pallas_call(step_kernel, out_shape=(jax.ShapeDtypeStruct((CHANNELS, HI...  116 us
    pallas_call x1, Pallas kernels, handed_on(): pl.pallas_call(hand_on_kernel, out_shape=tuple((jax.ShapeDtypeStruct(a.sh...  3.18 us

profile of v4, /device:TPU:2, one launch (start us, length us, event | category | flops | bytes accessed | tf_op | source)
XLA Modules:
  0.0 120.2 jit_solution(5211853256367020052)
XLA Ops:
  0.6 116.2 %step.1 = (bf16[2048,256]{1,0:T(8,128)(2,1)}, bf16[2048,256]{1,0:T(8,128)(2,1)}, bf16[256,2048]{1,0:T(8,128)(2,1)}, f32[8,2048]{1,0:T(8,128)}, bf16[256,512]{1,0:T(8,128)(2,1)}, /*index=5*/bf16[256,512]{1,0:T(8,128)(2,1)}) custom-call(bf16[256,512]{1,0:T(8,128)(2,1)} %cot.1, s32[2,256]{1,0:T(2,128)} %bitcast.14, f32[2,256]{1,0:T(2,128)} %bitcast.15, ...), custom_call_target="tpu_custom_call" | custom-call | tf_op jit(solution)/shard_map/step/pallas_call | solution.py:644
  116.9 3.2 %handed_on.1 = (bf16[2048,256]{1,0:T(8,128)(2,1)}, bf16[2048,256]{1,0:T(8,128)(2,1)}, bf16[256,2048]{1,0:T(8,128)(2,1)}, f32[8,2048]{1,0:T(8,128)}, bf16[256,512]{1,0:T(8,128)(2,1)}, /*index=5*/bf16[256,512]{1,0:T(8,128)(2,1)}) custom-call(bf16[2048,256]{1,0:T(8,128)(2,1)} %get-tuple-element.18.refs_0_, bf16[2048,256]{1,0:T(8,128)(2,1)} %get-tuple-element.19.refs_1_, ...), custom_call_target="tpu_custom_call" | custom-call | tf_op jit(solution)/shard_map/handed_on/pallas_call | solution.py:610
